TPU v7x, 32 devices: a whole 2x2x4 slice. The times are simulated.
32 devices in a mesh: sp: 8 (over z, y), tp: 4 (over x, core).
Axes of the slice: x: 2, y: 2, z: 4, core: 2. Of those that a mesh axis runs over, the one named last changes fastest.
Arguments:
- tokens: bfloat16 [4096, 2048], P('sp'), may hold values from -24 to 24
- w_query: bfloat16 [2048, 1536], P('sp', 'tp'), as said below
- w_key: bfloat16 [2048, 1536], P('sp', 'tp'), as said below
- w_value: bfloat16 [2048, 1536], P('sp', 'tp'), may hold values from -0.125 to 0.125
- w_out: bfloat16 [512, 2048], P('tp', 'sp'), may hold values from -1.5 to 1.5
Outputs:
- mixed: bfloat16 [4096, 2048], P(('sp', 'tp'))
Inputs may be any that keep to these rules, and one draw needn't show every extreme that they name: `w_query`: every entry lies within 4 / sqrt(2048) of zero. `w_key`: every entry lies within 4 / sqrt(2048) of zero.
All inputs are finite; a program needn't handle non-finite values.
Results may differ from a plain program's by a relative error of at most 0.025.
Values may be sent and summed in bfloat16 or wider, within the bound.
A program may use at most 64 MiB of HBM per device.

v0:
```python
import functools
import math

import jax
import jax.numpy as jnp
from jax import lax
from jax.experimental import pallas as pl
from jax.experimental.pallas import tpu as pltpu
from jax.sharding import PartitionSpec as P

GROUPS = 3
DH = 128
WIN1 = 128
WIN2 = 512
WIN3 = 2048
SECOND_DILATION = 4
THIRD_DILATION = 16


ROPE_BASE = 500000.0


def from_behind(block, axis, distance):
    devices = range(lax.axis_size(axis))
    route = [(i - distance, i) for i in devices if i - distance in devices]
    return lax.ppermute(block, axis, route)


def rotate(projected, offset):
    tok_rows = projected.shape[0]
    head_size = projected.shape[-1]
    half_size = head_size // 2
    positions = (offset + jnp.arange(tok_rows, dtype=jnp.int32)).astype(jnp.float32)
    frequency = 1.0 / ROPE_BASE ** (jnp.arange(0, head_size, 2, dtype=jnp.float32) / head_size)
    angles = (positions[:, None] * frequency[None, :]).reshape(tok_rows, 1, 1, half_size)
    cosine = jnp.cos(angles)
    sine_part = jnp.sin(angles)
    first_half = projected[..., :half_size]
    second_half = projected[..., half_size:]
    return jnp.concatenate(
        [
            first_half * cosine - second_half * sine_part,
            second_half * cosine + first_half * sine_part,
        ],
        axis=-1,
    )


def window_attend(query_part, buffer, steps, stride, offset):
    tok_rows, heads_here, head_size = query_part.shape
    sub_rows = tok_rows // stride
    key_rows = buffer.shape[1] // stride
    query_sub = query_part.reshape(sub_rows, stride, heads_here, head_size).transpose(1, 2, 0, 3)
    pair_sub = buffer.reshape(2, key_rows, stride, heads_here, head_size).transpose(0, 2, 3, 1, 4)
    block_rows = math.gcd(sub_rows, steps) if sub_rows > steps else sub_rows
    block_list = sub_rows // block_rows
    query_blocks = query_sub.reshape(stride, heads_here, block_list, block_rows, head_size)
    key_blocks = jnp.stack(
        [
            pair_sub[:, :, :, index * block_rows : index * block_rows + block_rows + steps]
            for index in range(block_list)
        ],
        axis=3,
    )
    scores = jnp.einsum(
        "zhnqe,zhnke->zhnqk", query_blocks, key_blocks[0], preferred_element_type=jnp.float32
    ) * head_size ** (-0.5)
    query_index = (jnp.arange(block_list, dtype=jnp.int32) * block_rows)[
        :, None, None
    ] + jnp.arange(block_rows, dtype=jnp.int32)[None, :, None]
    key_index = (jnp.arange(block_list, dtype=jnp.int32) * block_rows)[:, None, None] + jnp.arange(
        block_rows + steps, dtype=jnp.int32
    )[None, None, :]
    spacing = query_index + steps - key_index
    residue = jnp.arange(stride, dtype=jnp.int32)[:, None, None, None]
    key_position = offset + (key_index[None] - steps) * stride + residue
    allowed = (spacing[None] >= 0) & (spacing[None] <= steps) & (key_position >= 0)
    scores = jnp.where(allowed[:, None], scores, -jnp.inf)
    row_max = jnp.max(scores, axis=-1)
    exponent = jnp.exp(scores - row_max[..., None])
    totals = jnp.sum(exponent, axis=-1)
    probs = (exponent / totals[..., None]).astype(jnp.bfloat16)
    mixed = jnp.einsum(
        "zhnqk,zhnke->zhnqe", probs, key_blocks[1], preferred_element_type=jnp.float32
    )
    mixed = mixed.reshape(stride, heads_here, sub_rows, head_size).transpose(2, 0, 1, 3)
    log_total = (row_max + jnp.log(totals)).reshape(stride, heads_here, sub_rows).transpose(2, 0, 1)
    return (mixed.reshape(tok_rows, heads_here, head_size), log_total.reshape(tok_rows, heads_here))


def reach_back(key_value, distance_max):
    tok_rows = key_value.shape[1]
    gathered = key_value
    pieces_held = 1
    while pieces_held < distance_max + 1:
        slice_share = min(pieces_held, distance_max + 1 - pieces_held)
        arrived = from_behind(
            gathered[:, gathered.shape[1] - slice_share * tok_rows :], "sp", pieces_held
        )
        gathered = jnp.concatenate([arrived, gathered], axis=1)
        pieces_held = pieces_held + slice_share
    return gathered


def on_device(tokens, w_query, w_key, w_value, w_out):
    tok_rows = tokens.shape[0]
    heads_here = w_out.shape[0] // DH
    offset = lax.axis_index("sp") * tok_rows
    weight_parts = (
        lax.all_gather(w_query, "sp", axis=0, tiled=True),
        lax.all_gather(w_key, "sp", axis=0, tiled=True),
        lax.all_gather(w_value, "sp", axis=0, tiled=True),
    )
    query_raw, key_raw, value_raw = tuple(
        (
            jnp.dot(tokens, weight_rows, preferred_element_type=jnp.float32)
            for weight_rows in weight_parts
        )
    )
    head_shape = (tok_rows, heads_here, GROUPS, DH)
    queries = rotate(query_raw.reshape(head_shape), offset).astype(jnp.bfloat16)
    keys_all = rotate(key_raw.reshape(head_shape), offset).astype(jnp.bfloat16)
    values_all = value_raw.astype(jnp.bfloat16).reshape(head_shape)
    windows = (WIN1, WIN2, WIN3)
    step_sizes = (1, SECOND_DILATION, THIRD_DILATION)
    outputs = []
    log_totals = []
    for group_index in range(GROUPS):
        key_value = jnp.stack([keys_all[:, :, group_index], values_all[:, :, group_index]])
        key_value = key_value.reshape(2, tok_rows, heads_here * DH)
        window = windows[group_index]
        if group_index == 0:
            near_rows = from_behind(key_value[:, tok_rows - window :], "sp", 1)
            buffer = jnp.concatenate([near_rows, key_value], axis=1)
        else:
            distance_max = (window + tok_rows - 1) // tok_rows
            buffer = reach_back(key_value, distance_max)
        group_out, log_total = window_attend(
            queries[:, :, group_index],
            buffer,
            window // step_sizes[group_index],
            step_sizes[group_index],
            offset,
        )
        outputs.append(group_out)
        log_totals.append(log_total)
    group_weights = jax.nn.softmax(jnp.stack(log_totals), axis=0)
    merged = jnp.sum(group_weights[..., None] * jnp.stack(outputs), axis=0).astype(jnp.bfloat16)
    merged = merged.reshape(tok_rows, heads_here * DH)
    w_whole = lax.all_gather(w_out, "sp", axis=1, tiled=True)
    return lax.psum_scatter(
        jnp.dot(merged, w_whole, preferred_element_type=jnp.float32).astype(jnp.bfloat16),
        "tp",
        scatter_dimension=0,
        tiled=True,
    )


def layer_kernel(
    nz,
    tokens, w_key, w_value, w_query, w_out, out,
    weights, tok_in, tok_turned, cosine, sine, queries, pair0, send1, near1, far2,
    out_rows, mine, heads_in, got01, top01, sum01,
    swap_s, tok_r, w_r, up_s, down_s, side_s, o_r, o_s, o_r2, far_s, far_r, near_s, near_r, head_s, head_r,
):
    tok_rows, depth = tokens.shape
    k_rows, cols = w_key.shape
    sub = tok_rows // THIRD_DILATION
    sub_log = sub.bit_length() - 1
    block = tok_rows // SECOND_DILATION
    tail = WIN1
    sp, tp = lax.axis_index("sp"), lax.axis_index("tp")
    z, y = sp // 2, sp % 2
    x, c = tp // 2, tp % 2
    rank = 2 * z + c
    side = (sp, 2 * x + 1 - c)
    above = (sp + 2, tp)
    below = (sp - 2, tp)
    partner = (2 * z + 1 - y, 2 * x + 1 - c)
    stays = c == y
    has_up, has_down = z < nz - 1, z > 0

    def send(src, dst, s_sem, r_sem, where):
        return pltpu.make_async_remote_copy(
            src_ref=src, dst_ref=dst, send_sem=s_sem, recv_sem=r_sem,
            device_id=where, device_id_type=pl.DeviceIdType.MESH,
        )

    parts = (w_key, w_value, w_query)

    def chunk(a, s):
        return weights.at[a, pl.ds(pl.multiple_of(s * k_rows, k_rows), k_rows), :]

    def o_chunk(zz):
        return out_rows.at[c, x, y, zz]

    def swapped(a):
        there = 2 * z + 1 - c
        return send(parts[a], chunk(a, there), swap_s.at[a], w_r.at[a, there], partner)

    def tok_swapped():
        return send(tokens, tok_in, swap_s.at[3], tok_r, partner)

    def kept(a):
        return pltpu.make_async_copy(parts[a], chunk(a, rank), w_r.at[a, rank])

    def o_kept():
        return pltpu.make_async_copy(w_out, o_chunk(z), o_r.at[z])

    def tok_kept():
        return pltpu.make_async_copy(tokens, tok_in, tok_r)

    @pl.when(stays)
    def _():
        for a in range(3):
            kept(a).start()
        tok_kept().start()

    o_kept().start()

    barrier = pltpu.get_barrier_semaphore()

    def greet(where):
        pl.semaphore_signal(barrier, inc=1, device_id=where, device_id_type=pl.DeviceIdType.MESH)

    for dy in range(2):
        for dx in range(2):
            for dc in range(2):
                if dy + dx + dc:
                    greet((2 * z + (y + dy) % 2, 2 * ((x + dx) % 2) + (c + dc) % 2))
    pl.when(has_up)(lambda: greet(above))
    pl.when(has_down)(lambda: greet(below))
    pl.when(has_up & (c == 1))(lambda: greet((sp + 2, 2 * x)))
    pl.when(has_down & (c == 0))(lambda: greet((sp - 2, 2 * x + 1)))
    greeters = 7 + jnp.where(has_up, 1 + c, 0) + jnp.where(has_down, 2 - c, 0)
    pl.semaphore_wait(barrier, greeters)

    @pl.when(jnp.logical_not(stays))
    def _():
        swapped(0).start()
        swapped(1).start()
        tok_swapped().start()
        swapped(2).start()

    def go(a, zz, kind):
        s = 2 * zz + c
        ref = chunk(a, s) if a < 3 else o_chunk(zz)
        r_sem = w_r.at[a, s] if a < 3 else o_r.at[zz]
        s_sem = {"up": up_s, "down": down_s, "side": side_s}[kind].at[a, zz]
        return send(ref, ref, s_sem, r_sem, {"up": above, "down": below, "side": side}[kind])

    def own(a):
        if a < 3:
            pl.when(stays)(lambda: kept(a).wait())
            pl.when(jnp.logical_not(stays))(lambda: go(a, z, "side").wait_recv())
        else:
            o_kept().wait()
        pl.when(has_up)(lambda: go(a, z, "up").start())
        pl.when(has_down)(lambda: go(a, z, "down").start())
        if a < 3:
            go(a, z, "side").start()

    def relay(a, d):
        @pl.when(z - d >= 0)
        def _():
            go(a, z - d, "up").wait_recv()
            pl.when(has_up)(lambda: go(a, z - d, "up").start())
            if a < 3:
                go(a, z - d, "side").start()

        @pl.when(z + d < nz)
        def _():
            go(a, z + d, "down").wait_recv()
            pl.when(has_down)(lambda: go(a, z + d, "down").start())
            if a < 3:
                go(a, z + d, "side").start()

    def others(a):
        for zz in range(nz):
            s = 2 * zz + 1 - c
            send(chunk(a, s), chunk(a, s), side_s.at[a, zz], w_r.at[a, s], side).wait_recv()

    def row_time(p):
        b, i = p >> sub_log, p & (sub - 1)
        return THIRD_DILATION * i + (b >> 2) + SECOND_DILATION * (b & 3)

    def tail_time(u):
        per = tail // THIRD_DILATION
        b, i = u >> (per.bit_length() - 1), u & (per - 1)
        return THIRD_DILATION * (sub - per + i) + (b >> 2) + SECOND_DILATION * (b & 3) - tok_rows

    own(0)
    own(1)

    pair_at = lax.broadcasted_iota(jnp.int32, (1, DH), 1) & (DH // 2 - 1)
    freq = jnp.exp(pair_at.astype(jnp.float32) * (-2.0 * math.log(ROPE_BASE) / DH))

    def angles(index, carry):
        rows = pl.ds(pl.multiple_of(index * block, block), block)
        p = lax.broadcasted_iota(jnp.int32, (block, DH), 0) + index * block
        angle = (row_time(p) + rank * tok_rows).astype(jnp.float32) * freq
        lane = lax.broadcasted_iota(jnp.int32, (block, DH), 1)
        cosine[rows, :] = jnp.cos(angle)
        turned = jnp.sin(angle)
        sine[rows, :] = jnp.where(lane < DH // 2, -turned, turned)
        return carry

    lax.fori_loop(0, SECOND_DILATION, angles, 0)

    def relay_all(a, following):
        for d in range(1, nz):
            if d == nz - 1 and following is not None:
                own(following)
            relay(a, d)

    def order(source):
        p = row_time(lax.broadcasted_iota(jnp.int32, (tok_rows, tok_rows), 0))
        t = lax.broadcasted_iota(jnp.int32, (tok_rows, tok_rows), 1)
        pick = jnp.where(p == t, 1.0, 0.0).astype(jnp.bfloat16)

        def piece(index, carry):
            at = pl.ds(pl.multiple_of(index * 256, 256), 256)
            tok_turned[:, at] = jnp.dot(
                pick, source[:, at], preferred_element_type=jnp.float32
            ).astype(jnp.bfloat16)
            return carry

        lax.fori_loop(0, depth // 256, piece, 0)

    @pl.when(stays)
    def _():
        tok_kept().wait()
        order(tok_in)

    def o_y():
        return send(out_rows.at[c, x, y], out_rows.at[c, x, y], o_s.at[0], o_r2.at[0], (2 * z + 1 - y, tp))

    def o_x():
        return send(out_rows.at[c, x], out_rows.at[c, x], o_s.at[1], o_r2.at[1], (sp, 2 * (1 - x) + c))

    def o_c():
        return send(out_rows.at[c], out_rows.at[c], o_s.at[2], o_r2.at[2], side)

    relay_all(0, 3)
    relay_all(3, None)
    o_y().start()
    relay_all(1, 2)
    relay(2, 1)

    @pl.when(jnp.logical_not(stays))
    def _():
        tok_swapped().wait_recv()
        order(tok_in)

    def project(a, store):
        def piece(index, carry):
            rows = pl.ds(pl.multiple_of(index * block, block), block)
            raw = jnp.dot(tok_turned[rows, :], weights[a], preferred_element_type=jnp.float32)
            for g in range(GROUPS):
                part = raw[:, g * DH : (g + 1) * DH]
                if a != 1:
                    part = part * cosine[rows, :] + pltpu.roll(part, DH // 2, 1) * sine[rows, :]
                store(index, rows, g, part)
            return carry

        lax.fori_loop(0, SECOND_DILATION, piece, 0)

    def keep_pair(which):
        def store(index, rows, g, part):
            if g == 2:
                far2[0, which, rows, :] = part.astype(jnp.bfloat16)
            elif g == 1:
                send1[which, rows, :] = part.astype(jnp.bfloat16)
            else:
                pair0[which, rows, :] = part.astype(jnp.bfloat16)
                per = tail // THIRD_DILATION
                last = jnp.concatenate(
                    [part[b * sub + sub - per : (b + 1) * sub] for b in range(4)], axis=0
                )
                at = pl.ds(pl.multiple_of(tok_rows + index * 4 * per, 4 * per), 4 * per)
                send1[which, at, :] = last.astype(jnp.bfloat16)

        return store

    others(0)
    project(0, keep_pair(0))
    others(1)
    project(1, keep_pair(1))

    def far(index, src, dst, where):
        return send(far2.at[src], far2.at[dst], far_s.at[index], far_r.at[dst], where)

    def near(where):
        return send(send1, near1, near_s, near_r, where)

    up_other = (sp + 2, 2 * x)
    pl.when(has_up & (c == 1))(lambda: near(up_other).start())
    pl.when(has_up)(lambda: far(0, 0, 2, above).start())
    pl.when(c == 0)(lambda: near(side).start())
    pl.when(c == 0)(lambda: far(1, 0, 1, side).start())

    for d in range(1, 5):
        @pl.when(rank < d)
        def _(d=d):
            far2[d] = jnp.zeros(far2.shape[1:], far2.dtype)

    @pl.when(rank < 1)
    def _():
        near1[...] = jnp.zeros(near1.shape, near1.dtype)

    for d in range(2, nz):
        relay(2, d)
    @pl.when(has_down)
    def _():
        far(0, 0, 2, above).wait_recv()
        pl.when(has_up)(lambda: far(2, 2, 4, above).start())
        pl.when(c == 0)(lambda: far(3, 2, 3, side).start())
        pl.when(c == 1)(lambda: far(3, 2, 1, side).start())

    o_y().wait()
    o_x().start()
    others(2)

    def keep_query(index, rows, g, part):
        queries[g, rows, :] = part.astype(jnp.bfloat16)

    project(2, keep_query)

    scale = DH ** (-0.5)
    far_off = 1 << 24

    def dots(q, k):
        return lax.dot_general(q, k, (((1,), (1,)), ((), ())), preferred_element_type=jnp.float32)

    def iota(shape, axis):
        return lax.broadcasted_iota(jnp.int32, shape, axis)

    def soft(scores, time_q, time_k, reach, first):
        gap = time_q - jnp.where(time_k >= first, time_k, far_off)
        scores = jnp.where((gap >= 0) & (gap <= reach), scores * scale, -jnp.inf)
        top = jnp.max(scores, axis=-1, keepdims=True)
        weight = jnp.exp(scores - top)
        return top, jnp.sum(weight, axis=-1, keepdims=True), weight.astype(jnp.bfloat16)

    def near_groups(index, carry):
        begin = index * block
        rows = pl.ds(pl.multiple_of(begin, block), block)
        q = queries[0, rows, :]
        tails = pl.ds(tok_rows, tail)
        scores = jnp.concatenate([dots(q, near1[0, tails, :]), dots(q, pair0[0])], axis=1)
        lane = iota((1, tail + tok_rows), 1)
        time_k = jnp.where(lane < tail, tail_time(lane & (tail - 1)), row_time(lane - tail))
        time_q = row_time(iota((block, 1), 0) + begin)
        top0, sum0, weight = soft(scores, time_q, time_k, WIN1, -rank * tok_rows)
        got0 = jnp.dot(weight[:, :tail], near1[1, tails, :], preferred_element_type=jnp.float32)
        got0 += jnp.dot(weight[:, tail:], pair0[1], preferred_element_type=jnp.float32)
        q = queries[1, rows, :]
        scores = jnp.concatenate([dots(q, near1[0, rows, :]), dots(q, send1[0, rows, :])], axis=1)

        def step_of(place):
            return 4 * (place & (sub - 1)) + (place >> sub_log)

        lane = iota((1, 2 * block), 1)
        step_k = step_of(lane & (block - 1)) + jnp.where(lane < block, -block, 0)
        top1, sum1, weight = soft(
            scores, step_of(iota((block, 1), 0)), step_k, WIN2 // SECOND_DILATION, -rank * block
        )
        got1 = jnp.dot(weight[:, :block], near1[1, rows, :], preferred_element_type=jnp.float32)
        got1 += jnp.dot(weight[:, block:], send1[1, rows, :], preferred_element_type=jnp.float32)
        top = jnp.maximum(top0, top1)
        f0, f1 = jnp.exp(top0 - top), jnp.exp(top1 - top)
        got01[rows, :] = f0 * got0 + f1 * got1
        top01[rows, :] = top
        sum01[rows, :] = f0 * sum0 + f1 * sum1
        return carry

    def far_group(index, carry):
        begin = index * block
        rows = pl.ds(pl.multiple_of(begin, block), block)
        all_scores = []
        for b in range(4):
            here = pl.ds(pl.multiple_of(begin + b * sub, sub), sub)
            keys = jnp.concatenate([far2[d, 0, here, :] for d in (4, 3, 2, 1, 0)], axis=0)
            all_scores.append(dots(queries[2, here, :], keys))
        scores = jnp.concatenate(all_scores, axis=0)
        step_q = iota((block, 1), 0) & (sub - 1)
        step_k = iota((1, 5 * sub), 1) - 4 * sub
        top2, sum2, weight = soft(scores, step_q, step_k, WIN3 // THIRD_DILATION, -rank * sub)
        got = []
        for b in range(4):
            here = pl.ds(pl.multiple_of(begin + b * sub, sub), sub)
            vals = jnp.concatenate([far2[d, 1, here, :] for d in (4, 3, 2, 1, 0)], axis=0)
            got.append(jnp.dot(weight[b * sub : (b + 1) * sub], vals, preferred_element_type=jnp.float32))
        got2 = jnp.concatenate(got, axis=0)
        top1 = top01[rows, :]
        top = jnp.maximum(top1, top2)
        f1, f2 = jnp.exp(top1 - top), jnp.exp(top2 - top)
        total = f1 * sum01[rows, :] + f2 * sum2
        mine[0, rows, :] = ((f1 * got01[rows, :] + f2 * got2) / total).astype(jnp.bfloat16)
        return carry

    pl.when(rank >= 1)(lambda: near(side).wait_recv())
    lax.fori_loop(0, SECOND_DILATION, near_groups, 0)
    o_x().wait()
    o_c().start()

    @pl.when(z >= 2)
    def _():
        far(2, 2, 4, above).wait_recv()
        pl.when(c == 1)(lambda: far(4, 4, 3, side).start())

    pl.when(rank >= 1)(lambda: far(1, 0, 1, side).wait_recv())
    pl.when(rank >= 3)(lambda: far(4, 4, 3, side).wait_recv())
    lax.fori_loop(0, SECOND_DILATION, far_group, 0)

    t = iota((tok_rows, tok_rows), 0)
    p = row_time(iota((tok_rows, tok_rows), 1))
    mine[1] = jnp.dot(
        jnp.where(p == t, 1.0, 0.0).astype(jnp.bfloat16), mine[0], preferred_element_type=jnp.float32
    ).astype(jnp.bfloat16)
    head = 2 * x + y
    quarter = tok_rows // 4

    def deal(k):
        return send(mine.at[1, pl.ds(k * quarter, quarter), :], heads_in.at[head], head_s.at[k], head_r.at[head], (2 * z + c, k))

    def deal_self(k):
        return pltpu.make_async_copy(mine.at[1, pl.ds(k * quarter, quarter), :], heads_in.at[head], head_r.at[head])

    for k in range(4):
        self_here = (y == c) & (tp == k)
        pl.when(self_here)(lambda k=k: deal_self(k).start())
        pl.when(jnp.logical_not(self_here))(lambda k=k: deal(k).start())

    o_c().wait()
    for h in range(4):
        pltpu.make_async_copy(heads_in.at[h], heads_in.at[h], head_r.at[h]).wait()
    for zz in range(nz):
        for yy in range(2):
            acc = None
            for h in range(4):
                one = jnp.dot(heads_in[h], out_rows[h % 2, h // 2, yy, zz], preferred_element_type=jnp.float32)
                acc = one if acc is None else acc + one
            width = w_out.shape[1]
            s = 2 * zz + yy
            out[:, s * width : (s + 1) * width] = acc.astype(jnp.bfloat16)

    for k in range(4):
        self_here = (y == c) & (tp == k)
        pl.when(jnp.logical_not(self_here))(lambda k=k: deal(k).wait_send())

    @pl.when(jnp.logical_not(stays))
    def _():
        for a in range(3):
            swapped(a).wait_send()
        tok_swapped().wait_send()

    for a in range(4):
        for zz in range(nz):
            pl.when(has_up & (zz <= z))(lambda a=a, zz=zz: go(a, zz, "up").wait_send())
            pl.when(has_down & (zz >= z))(lambda a=a, zz=zz: go(a, zz, "down").wait_send())
            if a < 3:
                go(a, zz, "side").wait_send()
    pl.when(has_up)(lambda: far(0, 0, 2, above).wait_send())
    pl.when(c == 0)(lambda: far(1, 0, 1, side).wait_send())
    pl.when((c == 0) | has_up)(lambda: near(side).wait_send())
    pl.when(has_down & has_up)(lambda: far(2, 2, 4, above).wait_send())
    pl.when(has_down)(lambda: far(3, 2, 3, side).wait_send())
    pl.when((z >= 2) & (c == 1))(lambda: far(4, 4, 3, side).wait_send())


def fits_kernel(n_sp, n_tp, tokens, w_query, w_out):
    tok_rows, depth = tokens.shape
    return (
        n_sp % 2 == 0
        and n_tp == 4
        and w_query.shape[1] == GROUPS * DH
        and w_out.shape[0] == DH
        and w_out.shape[1] % 128 == 0
        and w_query.shape[0] % 16 == 0
        and tok_rows == WIN2
        and 4 * tok_rows == WIN3
        and 4 * WIN1 == tok_rows
    )


def one_kernel(n_sp, tokens, w_query, w_key, w_value, w_out):
    nz = n_sp // 2
    tok_rows, depth = tokens.shape
    cols = w_query.shape[1]
    bf, dma = jnp.bfloat16, pltpu.SemaphoreType.DMA
    return pl.pallas_call(
        functools.partial(layer_kernel, nz),
        out_shape=jax.ShapeDtypeStruct((tok_rows // 4, w_out.shape[1] * n_sp), bf),
        in_specs=[pl.BlockSpec(memory_space=pltpu.HBM)] * 5,
        out_specs=pl.BlockSpec(memory_space=pltpu.VMEM),
        scratch_shapes=[
            pltpu.VMEM((3, depth, cols), bf),
            pltpu.VMEM((tok_rows, depth), bf),
            pltpu.VMEM((tok_rows, depth), bf),
            pltpu.VMEM((tok_rows, DH), jnp.float32),
            pltpu.VMEM((tok_rows, DH), jnp.float32),
            pltpu.VMEM((GROUPS, tok_rows, DH), bf),
            pltpu.VMEM((2, tok_rows, DH), bf),
            pltpu.VMEM((2, tok_rows + WIN1, DH), bf),
            pltpu.VMEM((2, tok_rows + WIN1, DH), bf),
            pltpu.VMEM((5, 2, tok_rows, DH), bf),
            pltpu.VMEM((2, 2, 2, nz, *w_out.shape), bf),
            pltpu.VMEM((2, tok_rows, DH), bf),
            pltpu.VMEM((4, tok_rows // 4, DH), bf),
            pltpu.VMEM((tok_rows, DH), jnp.float32),
            pltpu.VMEM((tok_rows, 1), jnp.float32),
            pltpu.VMEM((tok_rows, 1), jnp.float32),
            dma((4,)), dma, dma((3, n_sp)),
            dma((4, nz)), dma((4, nz)), dma((3, nz)),
            dma((nz,)), dma((3,)), dma((3,)),
            dma((5,)), dma((5,)), dma, dma,
            dma((4,)), dma((4,)),
        ],
        compiler_params=pltpu.CompilerParams(
            collective_id=0, has_side_effects=True, vmem_limit_bytes=60 * 1024 * 1024
        ),
    )(tokens, w_key, w_value, w_query, w_out)


def on_mesh(n_sp, n_tp, *operands):
    tokens, w_query, _, _, w_out = operands
    if fits_kernel(n_sp, n_tp, tokens, w_query, w_out):
        return one_kernel(n_sp, *operands)
    return on_device(*operands)


def solution(mesh):
    placed = (P("sp", None), P("sp", "tp"), P("sp", "tp"), P("sp", "tp"), P("tp", "sp"))
    body = functools.partial(on_mesh, mesh.shape["sp"], mesh.shape["tp"])
    return jax.shard_map(
        body, mesh=mesh, in_specs=placed, out_specs=P(("sp", "tp"), None), check_vma=False
    )
```

profile of v0, /device:TPU:25, one launch (start us, length us, event | category | flops | bytes accessed | tf_op | source)
XLA Modules:
  0.0 78.7 jit_solution(5317819443790387477)
XLA Ops:
  0.0 76.8 %shard_map.55 = bf16[128,2048]{1,0:T(8,128)(2,1)} custom-call(bf16[512,2048]{1,0:T(8,128)(2,1)} %tokens.1, bf16[256,384]{1,0:T(8,128)(2,1)} %w_key.1, bf16[256,384]{1,0:T(8,128)(2,1)} %w_value.1, bf16[256,384]{1,0:T(8,128)(2,1)} %w_query.1, bf16[128,256]{1,0:T(8,128)(2,1)} %w_out.1), custom_call_target="tpu_custom_call" | custom-call | tf_op jit(solution)/shard_map/pallas_call | solution.py:592
  76.8 1.9 %copy.7 = bf16[128,2048]{1,0:T(8,128)(2,1)} copy(bf16[128,2048]{1,0:T(8,128)(2,1)} %shard_map.55) | data formatting | bytes 1048576
where the time goes:
time: 78.9 us; the launch traced here: 78.7 us
  Pallas kernels  76.8 us (97%)
  local copies, waits for them, and re-layouts  1.88 us (2%)
    pallas_call x1, Pallas kernels, one_kernel(): pl.pallas_call(functools.partial(layer_kernel, nz), out_shape=jax.ShapeDt...  76.8 us
    unnamed x1, local copies, waits for them, and re-layouts  1.88 us

commit v1 on v0

v1 whole, which is shorter than its diff:
```python
import functools
import math

import jax
import jax.numpy as jnp
from jax import lax
from jax.experimental import pallas as pl
from jax.experimental.pallas import tpu as pltpu
from jax.sharding import PartitionSpec as P

GROUPS = 3
DH = 128
WIN1 = 128
WIN2 = 512
WIN3 = 2048
SECOND_DILATION = 4
THIRD_DILATION = 16


ROPE_BASE = 500000.0

LAYERS = 4
TOKEN_PIECES = 4


def from_behind(block, axis, distance):
    devices = range(lax.axis_size(axis))
    route = [(i - distance, i) for i in devices if i - distance in devices]
    return lax.ppermute(block, axis, route)


def rotate(projected, offset):
    tok_rows = projected.shape[0]
    head_size = projected.shape[-1]
    half_size = head_size // 2
    positions = (offset + jnp.arange(tok_rows, dtype=jnp.int32)).astype(jnp.float32)
    frequency = 1.0 / ROPE_BASE ** (jnp.arange(0, head_size, 2, dtype=jnp.float32) / head_size)
    angles = (positions[:, None] * frequency[None, :]).reshape(tok_rows, 1, 1, half_size)
    cosine = jnp.cos(angles)
    sine_part = jnp.sin(angles)
    first_half = projected[..., :half_size]
    second_half = projected[..., half_size:]
    return jnp.concatenate(
        [
            first_half * cosine - second_half * sine_part,
            second_half * cosine + first_half * sine_part,
        ],
        axis=-1,
    )


def window_attend(query_part, buffer, steps, stride, offset):
    tok_rows, heads_here, head_size = query_part.shape
    sub_rows = tok_rows // stride
    key_rows = buffer.shape[1] // stride
    query_sub = query_part.reshape(sub_rows, stride, heads_here, head_size).transpose(1, 2, 0, 3)
    pair_sub = buffer.reshape(2, key_rows, stride, heads_here, head_size).transpose(0, 2, 3, 1, 4)
    block_rows = math.gcd(sub_rows, steps) if sub_rows > steps else sub_rows
    block_list = sub_rows // block_rows
    query_blocks = query_sub.reshape(stride, heads_here, block_list, block_rows, head_size)
    key_blocks = jnp.stack(
        [
            pair_sub[:, :, :, index * block_rows : index * block_rows + block_rows + steps]
            for index in range(block_list)
        ],
        axis=3,
    )
    scores = jnp.einsum(
        "zhnqe,zhnke->zhnqk", query_blocks, key_blocks[0], preferred_element_type=jnp.float32
    ) * head_size ** (-0.5)
    query_index = (jnp.arange(block_list, dtype=jnp.int32) * block_rows)[
        :, None, None
    ] + jnp.arange(block_rows, dtype=jnp.int32)[None, :, None]
    key_index = (jnp.arange(block_list, dtype=jnp.int32) * block_rows)[:, None, None] + jnp.arange(
        block_rows + steps, dtype=jnp.int32
    )[None, None, :]
    spacing = query_index + steps - key_index
    residue = jnp.arange(stride, dtype=jnp.int32)[:, None, None, None]
    key_position = offset + (key_index[None] - steps) * stride + residue
    allowed = (spacing[None] >= 0) & (spacing[None] <= steps) & (key_position >= 0)
    scores = jnp.where(allowed[:, None], scores, -jnp.inf)
    row_max = jnp.max(scores, axis=-1)
    exponent = jnp.exp(scores - row_max[..., None])
    totals = jnp.sum(exponent, axis=-1)
    probs = (exponent / totals[..., None]).astype(jnp.bfloat16)
    mixed = jnp.einsum(
        "zhnqk,zhnke->zhnqe", probs, key_blocks[1], preferred_element_type=jnp.float32
    )
    mixed = mixed.reshape(stride, heads_here, sub_rows, head_size).transpose(2, 0, 1, 3)
    log_total = (row_max + jnp.log(totals)).reshape(stride, heads_here, sub_rows).transpose(2, 0, 1)
    return (mixed.reshape(tok_rows, heads_here, head_size), log_total.reshape(tok_rows, heads_here))


def reach_back(key_value, distance_max):
    tok_rows = key_value.shape[1]
    gathered = key_value
    pieces_held = 1
    while pieces_held < distance_max + 1:
        slice_share = min(pieces_held, distance_max + 1 - pieces_held)
        arrived = from_behind(
            gathered[:, gathered.shape[1] - slice_share * tok_rows :], "sp", pieces_held
        )
        gathered = jnp.concatenate([arrived, gathered], axis=1)
        pieces_held = pieces_held + slice_share
    return gathered


def on_device(tokens, w_query, w_key, w_value, w_out):
    tok_rows = tokens.shape[0]
    heads_here = w_out.shape[0] // DH
    offset = lax.axis_index("sp") * tok_rows
    weight_parts = (
        lax.all_gather(w_query, "sp", axis=0, tiled=True),
        lax.all_gather(w_key, "sp", axis=0, tiled=True),
        lax.all_gather(w_value, "sp", axis=0, tiled=True),
    )
    query_raw, key_raw, value_raw = tuple(
        (
            jnp.dot(tokens, weight_rows, preferred_element_type=jnp.float32)
            for weight_rows in weight_parts
        )
    )
    head_shape = (tok_rows, heads_here, GROUPS, DH)
    queries = rotate(query_raw.reshape(head_shape), offset).astype(jnp.bfloat16)
    keys_all = rotate(key_raw.reshape(head_shape), offset).astype(jnp.bfloat16)
    values_all = value_raw.astype(jnp.bfloat16).reshape(head_shape)
    windows = (WIN1, WIN2, WIN3)
    step_sizes = (1, SECOND_DILATION, THIRD_DILATION)
    outputs = []
    log_totals = []
    for group_index in range(GROUPS):
        key_value = jnp.stack([keys_all[:, :, group_index], values_all[:, :, group_index]])
        key_value = key_value.reshape(2, tok_rows, heads_here * DH)
        window = windows[group_index]
        if group_index == 0:
            near_rows = from_behind(key_value[:, tok_rows - window :], "sp", 1)
            buffer = jnp.concatenate([near_rows, key_value], axis=1)
        else:
            distance_max = (window + tok_rows - 1) // tok_rows
            buffer = reach_back(key_value, distance_max)
        group_out, log_total = window_attend(
            queries[:, :, group_index],
            buffer,
            window // step_sizes[group_index],
            step_sizes[group_index],
            offset,
        )
        outputs.append(group_out)
        log_totals.append(log_total)
    group_weights = jax.nn.softmax(jnp.stack(log_totals), axis=0)
    merged = jnp.sum(group_weights[..., None] * jnp.stack(outputs), axis=0).astype(jnp.bfloat16)
    merged = merged.reshape(tok_rows, heads_here * DH)
    w_whole = lax.all_gather(w_out, "sp", axis=1, tiled=True)
    return lax.psum_scatter(
        jnp.dot(merged, w_whole, preferred_element_type=jnp.float32).astype(jnp.bfloat16),
        "tp",
        scatter_dimension=0,
        tiled=True,
    )


def layer_kernel(
    nz,
    tokens, w_key, w_value, w_query, w_out, out,
    weights, stage, tok_in, tok_turned, cosine, sine, queries, pair0, near_own, near_in, far2,
    out_rows, mine, heads_in, got01, top01, sum01,
    stage_s, swap_s, tok_k, w_r, mid_s, side_s, t_r, tz_s, ty_s, tx_s,
    up_s, down_s, o_r, o_s, o_r2, far_s, far_r, near_s, near_r, head_s, head_r,
):
    tok_rows, depth = tokens.shape
    k_rows, cols = w_key.shape
    sub = tok_rows // THIRD_DILATION
    sub_log = sub.bit_length() - 1
    block = tok_rows // SECOND_DILATION
    tail = WIN1
    pieces = tz_s.shape[0]
    piece_rows = tok_rows // 2 // pieces
    sp, tp = lax.axis_index("sp"), lax.axis_index("tp")
    z, y = sp // 2, sp % 2
    x, c = tp // 2, tp % 2
    last = nz - 1
    is_mid = (z == 1) | (z == 2)
    is_end = jnp.logical_not(is_mid)
    stays = c == y
    moves = jnp.logical_not(stays)
    has_up, has_down = z < last, z > 0
    other = last - z
    end = jnp.where(z == 1, 0, last)
    far_end = last - end
    hub = jnp.where(z == 0, 1, 2)
    j_own = jnp.where(z == 1, 1, 0)
    j_far = 1 - j_own
    j_end = jnp.where(z == 0, 0, 1)
    base = 4 * (z - 1)
    side = (sp, 2 * x + 1 - c)
    across_x = (sp, 2 * (1 - x) + c)
    across_y = (2 * z + 1 - y, tp)
    partner = (2 * z + 1 - y, 2 * x + 1 - c)
    above, below = (sp + 2, tp), (sp - 2, tp)
    opposite = (2 * other + y, tp)
    to_hub = (2 * hub + y, tp)

    def send(src, dst, s_sem, r_sem, where):
        return pltpu.make_async_remote_copy(
            src_ref=src, dst_ref=dst, send_sem=s_sem, recv_sem=r_sem,
            device_id=where, device_id_type=pl.DeviceIdType.MESH,
        )

    parts = (w_key, w_value, w_query)

    def chunk(a, s):
        return weights.at[a, pl.ds(pl.multiple_of(s * k_rows, k_rows), k_rows), :]

    def put_w(a, zz, s_sem, where):
        s = 2 * zz + c
        return send(chunk(a, s), chunk(a, s), s_sem, w_r.at[a, s], where)

    def arrived(a, zz):
        put_w(a, zz, side_s.at[a, 0], side).wait_recv()

    def kept(a):
        return pltpu.make_async_copy(parts[a], chunk(a, 2 * z + c), w_r.at[a, 2 * z + c])

    def staged(a):
        return pltpu.make_async_copy(parts[a], stage.at[a], stage_s.at[a])

    def swapped(a):
        there = 2 * z + 1 - c
        return send(stage.at[a], chunk(a, there), swap_s.at[a], w_r.at[a, there], partner)

    def o_chunk(zz):
        return out_rows.at[c, y, x, zz]

    def o_kept():
        return pltpu.make_async_copy(w_out, o_chunk(z), o_r.at[z])

    tok_slot = jnp.where(is_mid, j_own, j_end)

    def tok_kept():
        return pltpu.make_async_copy(tokens, tok_in.at[tok_slot], tok_k)

    o_kept().start()

    @pl.when(stays)
    def _():
        for a in range(3):
            kept(a).start()
        tok_kept().start()

    @pl.when(moves)
    def _():
        for a in range(3):
            staged(a).start()

    barrier = pltpu.get_barrier_semaphore()

    def greet(where):
        pl.semaphore_signal(barrier, inc=1, device_id=where, device_id_type=pl.DeviceIdType.MESH)

    paired = z + 1 - 2 * (z % 2)
    for dy in range(2):
        for dx in range(2):
            for dc in range(2):
                where = ((y + dy) % 2, 2 * ((x + dx) % 2) + (c + dc) % 2)
                if dy + dx + dc:
                    greet((2 * z + where[0], where[1]))
                greet((2 * paired + where[0], where[1]))

    @pl.when(is_mid)
    def _():
        greet(opposite)
        greet((2 * other + y, 2 * x + 1 - c))

    pl.semaphore_wait(barrier, 15 + jnp.where(is_mid, 2, 0))

    pl.when(moves)(lambda: staged(0).wait())
    pl.when(moves)(lambda: swapped(0).start())

    def o_go(zz, kind):
        ref = o_chunk(zz)
        s_sem, where = {"up": (up_s, above), "down": (down_s, below)}[kind]
        return send(ref, ref, s_sem.at[zz], o_r.at[zz], where)

    def o_relay(d):
        @pl.when(z - d >= 0)
        def _():
            o_go(z - d, "up").wait_recv()
            pl.when(has_up)(lambda: o_go(z - d, "up").start())

        @pl.when(z + d < nz)
        def _():
            o_go(z + d, "down").wait_recv()
            pl.when(has_down)(lambda: o_go(z + d, "down").start())

    def o_share(axis):
        ref, where = (
            (out_rows.at[c, y, x], across_x),
            (out_rows.at[c, y], across_y),
            (out_rows.at[c], side),
        )[axis]
        return send(ref, ref, o_s.at[axis], o_r2.at[axis], where)

    def t_piece(j, half, q):
        at = half * (tok_rows // 2) + q * piece_rows
        return tok_in.at[j, pl.ds(pl.multiple_of(at, piece_rows), piece_rows), :]

    def put_t(j, half, q, s_sem, where):
        ref = t_piece(j, half, q)
        return send(ref, ref, s_sem, t_r.at[j, half, q], where)

    def t_inward(q):
        return put_t(j_end, x, q, tz_s.at[q], to_hub)

    def t_y(j, q):
        return put_t(j, x, q, ty_s.at[j, q], across_y)

    def t_x(j, q):
        return put_t(j, x, q, tx_s.at[j, q], across_x)

    def t_other(j):
        for q in range(pieces):
            put_t(j, 1 - x, q, tx_s.at[j, q], across_x).wait_recv()

    def w_inward(a):
        return put_w(a, z, mid_s.at[a, 0], to_hub)

    def w_cross(a, which):
        return put_w(a, (z, end)[which], mid_s.at[a, which], opposite)

    ring = (z, end, other, far_end)

    def w_side(a, which):
        return put_w(a, ring[which], side_s.at[a, which], side)

    def own_ready(a):
        pl.when(stays)(lambda: kept(a).wait())
        pl.when(moves)(lambda: arrived(a, z))

    o_kept().wait()
    pl.when(has_up)(lambda: o_go(z, "up").start())
    pl.when(has_down)(lambda: o_go(z, "down").start())

    def rest_swapped():
        for a in (1, 2):
            staged(a).wait()
            swapped(a).start()

    @pl.when(is_end)
    def _():
        @pl.when(stays)
        def _():
            kept(0).wait()
            w_inward(0).start()
            tok_kept().wait()
            t_inward(0).start()
            kept(1).wait()
            w_inward(1).start()
            t_inward(1).start()
            kept(2).wait()
            w_inward(2).start()
            for q in range(2, pieces):
                t_inward(q).start()

        pl.when(moves)(rest_swapped)
        o_relay(1)

        @pl.when(moves)
        def _():
            for a in range(3):
                arrived(a, z)
                w_inward(a).start()

        for d in range(2, nz):
            o_relay(d)
        o_share(0).start()
        o_share(0).wait()
        o_share(1).start()
        o_share(1).wait()
        o_share(2).start()

    def row_time(p):
        b, i = p >> sub_log, p & (sub - 1)
        return THIRD_DILATION * i + (b >> 2) + SECOND_DILATION * (b & 3)

    def tail_time(u):
        per = tail // THIRD_DILATION
        b, i = u >> (per.bit_length() - 1), u & (per - 1)
        return THIRD_DILATION * (sub - per + i) + (b >> 2) + SECOND_DILATION * (b & 3) - tok_rows

    def iota(shape, axis):
        return lax.broadcasted_iota(jnp.int32, shape, axis)

    def angles(index, carry):
        j, at = index // SECOND_DILATION, (index % SECOND_DILATION) * block
        rows = pl.ds(pl.multiple_of(at, block), block)
        pair_at = iota((1, DH), 1) & (DH // 2 - 1)
        freq = jnp.exp(pair_at.astype(jnp.float32) * (-2.0 * math.log(ROPE_BASE) / DH))
        first = (base + 2 * j + c) * tok_rows
        angle = (row_time(iota((block, DH), 0) + at) + first).astype(jnp.float32) * freq
        cosine[j, rows, :] = jnp.cos(angle)
        turned = jnp.sin(angle)
        sine[j, rows, :] = jnp.where(iota((block, DH), 1) < DH // 2, -turned, turned)
        return carry

    def order(j):
        p = row_time(iota((tok_rows, tok_rows), 0))
        t = iota((tok_rows, tok_rows), 1)
        pick = jnp.where(p == t, 1.0, 0.0).astype(jnp.bfloat16)

        def piece(index, carry):
            at = pl.ds(pl.multiple_of(index * 256, 256), 256)
            tok_turned[j, :, at] = jnp.dot(
                pick, tok_in[j, :, at], preferred_element_type=jnp.float32
            ).astype(jnp.bfloat16)
            return carry

        lax.fori_loop(0, depth // 256, piece, 0)

    def project(j, a, store):
        def piece(index, carry):
            rows = pl.ds(pl.multiple_of(index * block, block), block)
            raw = jnp.dot(tok_turned[j, rows, :], weights[a], preferred_element_type=jnp.float32)
            for g in range(GROUPS):
                part = raw[:, g * DH : (g + 1) * DH]
                if a != 1:
                    part = part * cosine[j, rows, :] + pltpu.roll(part, DH // 2, 1) * sine[j, rows, :]
                store(index, rows, g, part)
            return carry

        lax.fori_loop(0, SECOND_DILATION, piece, 0)

    def keep_pair(j, which):
        def store(index, rows, g, part):
            if g == 2:
                far2[4 + 2 * j + c, which, rows, :] = part.astype(jnp.bfloat16)
            elif g == 1:
                near_own[j, which, rows, :] = part.astype(jnp.bfloat16)
            else:
                pair0[j, which, rows, :] = part.astype(jnp.bfloat16)
                per = tail // THIRD_DILATION
                ends = jnp.concatenate(
                    [part[b * sub + sub - per : (b + 1) * sub] for b in range(4)], axis=0
                )
                at = pl.ds(pl.multiple_of(tok_rows + index * 4 * per, 4 * per), 4 * per)
                near_own[j, which, at, :] = ends.astype(jnp.bfloat16)

        return store

    def keep_query(j):
        def store(index, rows, g, part):
            queries[j, g, rows, :] = part.astype(jnp.bfloat16)

        return store

    def others(a):
        for zz in range(nz):
            s = 2 * zz + 1 - c
            send(chunk(a, s), chunk(a, s), side_s.at[a, 0], w_r.at[a, s], side).wait_recv()

    def far(kind, src, dst, where):
        return send(far2.at[src], far2.at[dst], far_s.at[kind], far_r.at[dst], where)

    def far_side(j):
        return far(j, 4 + 2 * j + c, 4 + 2 * j + c, side)

    def far_up(j):
        return far(2 + j, 4 + 2 * j + c, 2 * j + c, above)

    def far_pass(j):
        return far(4 + j, 2 * j + c, 2 * j + c, side)

    def near(j, dst, where):
        return send(near_own.at[j], near_in.at[dst], near_s.at[j], near_r.at[dst], where)

    up_other = (sp + 2, 2 * x)

    def halos(j):
        @pl.when((c == 1) & (j == 1) & (z == 1))
        def _():
            near(1, 0, up_other).start()

        pl.when(z == 1)(lambda: far_up(j).start())
        pl.when(c == 0)(lambda: near(j, j, side).start())
        pl.when((c == 1) & (j == 0))(lambda: near(0, 1, side).start())
        pl.when((c == 0) | (j == 0))(lambda: far_side(j).start())

    scale = DH ** (-0.5)
    far_off = 1 << 24

    def dots(q, k):
        return lax.dot_general(q, k, (((1,), (1,)), ((), ())), preferred_element_type=jnp.float32)

    def soft(scores, time_q, time_k, reach, first):
        gap = time_q - jnp.where(time_k >= first, time_k, far_off)
        scores = jnp.where((gap >= 0) & (gap <= reach), scores * scale, -jnp.inf)
        top = jnp.max(scores, axis=-1, keepdims=True)
        weight = jnp.exp(scores - top)
        return top, jnp.sum(weight, axis=-1, keepdims=True), weight.astype(jnp.bfloat16)

    def near_groups(j):
        rank = base + 2 * j + c

        def piece(index, carry):
            begin = index * block
            rows = pl.ds(pl.multiple_of(begin, block), block)
            q = queries[j, 0, rows, :]
            tails = pl.ds(tok_rows, tail)
            scores = jnp.concatenate([dots(q, near_in[j, 0, tails, :]), dots(q, pair0[j, 0])], axis=1)
            lane = iota((1, tail + tok_rows), 1)
            time_k = jnp.where(lane < tail, tail_time(lane & (tail - 1)), row_time(lane - tail))
            time_q = row_time(iota((block, 1), 0) + begin)
            top0, sum0, weight = soft(scores, time_q, time_k, WIN1, -rank * tok_rows)
            got0 = jnp.dot(weight[:, :tail], near_in[j, 1, tails, :], preferred_element_type=jnp.float32)
            got0 += jnp.dot(weight[:, tail:], pair0[j, 1], preferred_element_type=jnp.float32)
            q = queries[j, 1, rows, :]
            scores = jnp.concatenate(
                [dots(q, near_in[j, 0, rows, :]), dots(q, near_own[j, 0, rows, :])], axis=1
            )

            def step_of(place):
                return 4 * (place & (sub - 1)) + (place >> sub_log)

            lane = iota((1, 2 * block), 1)
            step_k = step_of(lane & (block - 1)) + jnp.where(lane < block, -block, 0)
            top1, sum1, weight = soft(
                scores, step_of(iota((block, 1), 0)), step_k, WIN2 // SECOND_DILATION, -rank * block
            )
            got1 = jnp.dot(weight[:, :block], near_in[j, 1, rows, :], preferred_element_type=jnp.float32)
            got1 += jnp.dot(weight[:, block:], near_own[j, 1, rows, :], preferred_element_type=jnp.float32)
            top = jnp.maximum(top0, top1)
            f0, f1 = jnp.exp(top0 - top), jnp.exp(top1 - top)
            got01[j, rows, :] = f0 * got0 + f1 * got1
            top01[j, rows, :] = top
            sum01[j, rows, :] = f0 * sum0 + f1 * sum1
            return carry

        lax.fori_loop(0, SECOND_DILATION, piece, 0)

    def far_group(j):
        rank = base + 2 * j + c
        slots = [4 + 2 * j + c - d for d in (4, 3, 2, 1, 0)]

        def piece(index, carry):
            begin = index * block
            rows = pl.ds(pl.multiple_of(begin, block), block)
            all_scores = []
            for b in range(4):
                here = pl.ds(pl.multiple_of(begin + b * sub, sub), sub)
                keys = jnp.concatenate([far2[s, 0, here, :] for s in slots], axis=0)
                all_scores.append(dots(queries[j, 2, here, :], keys))
            scores = jnp.concatenate(all_scores, axis=0)
            step_q = iota((block, 1), 0) & (sub - 1)
            step_k = iota((1, 5 * sub), 1) - 4 * sub
            top2, sum2, weight = soft(scores, step_q, step_k, WIN3 // THIRD_DILATION, -rank * sub)
            got = []
            for b in range(4):
                here = pl.ds(pl.multiple_of(begin + b * sub, sub), sub)
                vals = jnp.concatenate([far2[s, 1, here, :] for s in slots], axis=0)
                got.append(
                    jnp.dot(weight[b * sub : (b + 1) * sub], vals, preferred_element_type=jnp.float32)
                )
            got2 = jnp.concatenate(got, axis=0)
            top1 = top01[j, rows, :]
            top = jnp.maximum(top1, top2)
            f1, f2 = jnp.exp(top1 - top), jnp.exp(top2 - top)
            total = f1 * sum01[j, rows, :] + f2 * sum2
            mine[2, rows, :] = ((f1 * got01[j, rows, :] + f2 * got2) / total).astype(jnp.bfloat16)
            return carry

        lax.fori_loop(0, SECOND_DILATION, piece, 0)
        t = iota((tok_rows, tok_rows), 0)
        p = row_time(iota((tok_rows, tok_rows), 1))
        mine[j] = jnp.dot(
            jnp.where(p == t, 1.0, 0.0).astype(jnp.bfloat16), mine[2], preferred_element_type=jnp.float32
        ).astype(jnp.bfloat16)

    head = 2 * x + y
    quarter = tok_rows // 4

    def deal(j, k):
        return send(
            mine.at[j, pl.ds(k * quarter, quarter), :], heads_in.at[head], head_s.at[j, k], head_r.at[head],
            (base + 2 * j + c, k),
        )

    def deal_self(j, k):
        return pltpu.make_async_copy(mine.at[j, pl.ds(k * quarter, quarter), :], heads_in.at[head], head_r.at[head])

    def self_here(j, k):
        return (j == j_own) & stays & (tp == k)

    def deal_all(j):
        for k in range(4):
            pl.when(self_here(j, k))(lambda k=k: deal_self(j, k).start())
            pl.when(jnp.logical_not(self_here(j, k)))(lambda k=k: deal(j, k).start())

    @pl.when(is_mid)
    def _():
        @pl.when(stays)
        def _():
            kept(0).wait()
            w_cross(0, 0).start()
            w_side(0, 0).start()
            tok_kept().wait()
            for q in range(pieces):
                t_y(j_own, q).start()

        pl.when(moves)(rest_swapped)
        o_relay(1)
        lax.fori_loop(0, 2 * SECOND_DILATION, angles, 0)

        @pl.when(moves)
        def _():
            arrived(0, z)
            w_cross(0, 0).start()
            w_side(0, 0).start()

        def relay_end(a):
            arrived(a, end)
            w_cross(a, 1).start()
            w_side(a, 1).start()

        def relay_side(a, which):
            arrived(a, ring[which])
            w_side(a, which).start()

        def own_on(a):
            own_ready(a)
            w_cross(a, 0).start()
            w_side(a, 0).start()

        def far_on_stays(q):
            put_t(j_far, x, q, tz_s.at[q], to_hub).wait_recv()
            t_x(j_far, q).start()
            t_y(j_far, q).start()

        def on_moves(j, q):
            t_y(j, q).wait_recv()
            t_x(j, q).start()

        def advance(stay_list, move_list):
            @pl.when(stays)
            def _():
                for q in stay_list:
                    far_on_stays(q)

            @pl.when(moves)
            def _():
                for j, q in move_list:
                    on_moves(j, q)

        relay_end(0)
        own_on(1)
        o_relay(2)
        o_relay(3)
        o_share(0).start()
        advance([0], [(j_own, 0)])
        own_on(2)
        relay_side(0, 2)
        relay_side(0, 3)
        advance([], [(j_own, 1)])
        relay_end(1)
        o_share(0).wait()
        o_share(1).start()
        advance([1], [(j_own, 2), (j_own, 3)])
        relay_end(2)
        relay_side(1, 2)
        pl.when(moves)(lambda: t_other(j_own))
        order(j_own)
        others(0)
        project(j_own, 0, keep_pair(j_own, 0))
        advance([2], [(j_far, 0), (j_far, 1)])
        relay_side(2, 2)
        relay_side(1, 3)
        others(1)
        project(j_own, 1, keep_pair(j_own, 1))
        halos(j_own)
        advance([3], [(j_far, 2), (j_far, 3)])
        relay_side(2, 3)
        o_share(1).wait()
        o_share(2).start()

        @pl.when(z == 1)
        def _():
            for s in range(4):
                far2[s] = jnp.zeros(far2.shape[1:], far2.dtype)

        @pl.when((z == 1) & (c == 0))
        def _():
            near_in[0] = jnp.zeros(near_in.shape[1:], near_in.dtype)

        t_other(j_far)
        order(j_far)
        project(j_far, 0, keep_pair(j_far, 0))
        project(j_far, 1, keep_pair(j_far, 1))
        halos(j_far)
        others(2)
        project(j_own, 2, keep_query(j_own))

        @pl.when(z == 2)
        def _():
            far_up(1).wait_recv()
            far_pass(1).start()

        project(j_far, 2, keep_query(j_far))
        pl.when((z == 2) | (c == 1))(lambda: near(0, 0, side).wait_recv())
        near(1, 1, side).wait_recv()
        near_groups(0)
        near_groups(1)
        for j in range(2):
            pl.when((c == 1) | (j == 0))(lambda j=j: far(j, 4, 5 - c + 2 * j, side).wait_recv())

        @pl.when(z == 2)
        def _():
            far(4, 0, 3 - c, side).wait_recv()

        far_group(1)
        deal_all(1)

        @pl.when(z == 2)
        def _():
            far_up(0).wait_recv()
            pl.when(c == 1)(lambda: far_pass(0).start())
            pl.when(c == 0)(lambda: far(4, 0, 1, side).wait_recv())

        far_group(0)
        deal_all(0)

    o_share(2).wait()
    for h in range(4):
        pltpu.make_async_copy(heads_in.at[h], heads_in.at[h], head_r.at[h]).wait()
    for zz in range(nz):
        for yy in range(2):
            acc = None
            for h in range(4):
                one = jnp.dot(heads_in[h], out_rows[h % 2, yy, h // 2, zz], preferred_element_type=jnp.float32)
                acc = one if acc is None else acc + one
            width = w_out.shape[1]
            s = 2 * zz + yy
            out[:, s * width : (s + 1) * width] = acc.astype(jnp.bfloat16)

    @pl.when(moves)
    def _():
        for a in range(3):
            swapped(a).wait_send()

    for zz in range(nz):
        pl.when(has_up & (zz <= z))(lambda zz=zz: o_go(zz, "up").wait_send())
        pl.when(has_down & (zz >= z))(lambda zz=zz: o_go(zz, "down").wait_send())

    @pl.when(is_end)
    def _():
        for a in range(3):
            w_inward(a).wait_send()

        @pl.when(stays)
        def _():
            for q in range(pieces):
                t_inward(q).wait_send()

    @pl.when(is_mid)
    def _():
        for a in range(3):
            for which in range(2):
                w_cross(a, which).wait_send()
            for which in range(4):
                w_side(a, which).wait_send()
        for q in range(pieces):
            t_x(j_far, q).wait_send()

            @pl.when(stays)
            def _(q=q):
                t_y(j_own, q).wait_send()
                t_y(j_far, q).wait_send()

            pl.when(moves)(lambda q=q: t_x(j_own, q).wait_send())
        for j in range(2):
            pl.when(z == 1)(lambda j=j: far_up(j).wait_send())
            pl.when((c == 0) | (j == 0))(lambda j=j: far_side(j).wait_send())
            pl.when((c == 0) | (j == 0) | (z == 1))(lambda j=j: near(j, j, side).wait_send())
            pl.when((z == 2) & ((c == 1) | (j == 1)))(lambda j=j: far_pass(j).wait_send())
            for k in range(4):
                pl.when(jnp.logical_not(self_here(j, k)))(lambda j=j, k=k: deal(j, k).wait_send())


def fits_kernel(n_sp, n_tp, tokens, w_query, w_out):
    tok_rows, depth = tokens.shape
    return (
        n_sp == 2 * LAYERS
        and n_tp == 4
        and w_query.shape[1] == GROUPS * DH
        and w_out.shape[0] == DH
        and w_out.shape[1] % 128 == 0
        and w_query.shape[0] % 16 == 0
        and tok_rows == WIN2
        and 4 * tok_rows == WIN3
        and 4 * WIN1 == tok_rows
    )


def one_kernel(n_sp, tokens, w_query, w_key, w_value, w_out):
    nz = n_sp // 2
    tok_rows, depth = tokens.shape
    cols = w_query.shape[1]
    bf, dma = jnp.bfloat16, pltpu.SemaphoreType.DMA
    return pl.pallas_call(
        functools.partial(layer_kernel, nz),
        out_shape=jax.ShapeDtypeStruct((tok_rows // 4, w_out.shape[1] * n_sp), bf),
        in_specs=[pl.BlockSpec(memory_space=pltpu.HBM)] * 5,
        out_specs=pl.BlockSpec(memory_space=pltpu.VMEM),
        scratch_shapes=[
            pltpu.VMEM((3, depth, cols), bf),
            pltpu.VMEM((3, *w_query.shape), bf),
            pltpu.VMEM((2, tok_rows, depth), bf),
            pltpu.VMEM((2, tok_rows, depth), bf),
            pltpu.VMEM((2, tok_rows, DH), jnp.float32),
            pltpu.VMEM((2, tok_rows, DH), jnp.float32),
            pltpu.VMEM((2, GROUPS, tok_rows, DH), bf),
            pltpu.VMEM((2, 2, tok_rows, DH), bf),
            pltpu.VMEM((2, 2, tok_rows + WIN1, DH), bf),
            pltpu.VMEM((2, 2, tok_rows + WIN1, DH), bf),
            pltpu.VMEM((8, 2, tok_rows, DH), bf),
            pltpu.VMEM((2, 2, 2, nz, *w_out.shape), bf),
            pltpu.VMEM((3, tok_rows, DH), bf),
            pltpu.VMEM((4, tok_rows // 4, DH), bf),
            pltpu.VMEM((2, tok_rows, DH), jnp.float32),
            pltpu.VMEM((2, tok_rows, 1), jnp.float32),
            pltpu.VMEM((2, tok_rows, 1), jnp.float32),
            dma((3,)), dma((3,)), dma, dma((3, n_sp)), dma((3, 2)), dma((3, 4)),
            dma((2, 2, TOKEN_PIECES)), dma((TOKEN_PIECES,)), dma((2, TOKEN_PIECES)), dma((2, TOKEN_PIECES)),
            dma((nz,)), dma((nz,)), dma((nz,)), dma((3,)), dma((3,)),
            dma((6,)), dma((8,)), dma((2,)), dma((2,)), dma((2, 4)), dma((4,)),
        ],
        compiler_params=pltpu.CompilerParams(
            collective_id=0, has_side_effects=True, vmem_limit_bytes=60 * 1024 * 1024
        ),
    )(tokens, w_key, w_value, w_query, w_out)


def on_mesh(n_sp, n_tp, *operands):
    tokens, w_query, _, _, w_out = operands
    if fits_kernel(n_sp, n_tp, tokens, w_query, w_out):
        return one_kernel(n_sp, *operands)
    return on_device(*operands)


def solution(mesh):
    placed = (P("sp", None), P("sp", "tp"), P("sp", "tp"), P("sp", "tp"), P("tp", "sp"))
    body = functools.partial(on_mesh, mesh.shape["sp"], mesh.shape["tp"])
    return jax.shard_map(
        body, mesh=mesh, in_specs=placed, out_specs=P(("sp", "tp"), None), check_vma=False
    )
```

time: 78.9 us -> 91.7 us (1.16)
  the two profiles are of different devices: /device:TPU:25 before, /device:TPU:1 now
where the time goes in v1:
time: 91.7 us; the launch traced here: 91.5 us
  Pallas kernels  89.6 us (98%)
  local copies, waits for them, and re-layouts  1.88 us (2%)
    pallas_call x1, Pallas kernels, one_kernel(): pl.pallas_call(functools.partial(layer_kernel, nz), out_shape=jax.ShapeDt...  89.6 us
    unnamed x1, local copies, waits for them, and re-layouts  1.88 us

profile of v1, /device:TPU:1, one launch (start us, length us, event | category | flops | bytes accessed | tf_op | source)
XLA Modules:
  0.0 91.5 jit_solution(8264909069086826627)
XLA Ops:
  0.0 89.6 %shard_map.55 = bf16[128,2048]{1,0:T(8,128)(2,1)} custom-call(bf16[512,2048]{1,0:T(8,128)(2,1)} %tokens.1, bf16[256,384]{1,0:T(8,128)(2,1)} %w_key.1, bf16[256,384]{1,0:T(8,128)(2,1)} %w_value.1, bf16[256,384]{1,0:T(8,128)(2,1)} %w_query.1, bf16[128,256]{1,0:T(8,128)(2,1)} %w_out.1), custom_call_target="tpu_custom_call" | custom-call | tf_op jit(solution)/shard_map/pallas_call | solution.py:806
  89.6 1.9 %copy.7 = bf16[128,2048]{1,0:T(8,128)(2,1)} copy(bf16[128,2048]{1,0:T(8,128)(2,1)} %shard_map.55) | data formatting | bytes 1048576

commit v2 on v0

v2 whole, which is shorter than its diff:
```python
import functools
import math

import jax
import jax.numpy as jnp
from jax import lax
from jax.experimental import pallas as pl
from jax.experimental.pallas import tpu as pltpu
from jax.sharding import PartitionSpec as P

GROUPS = 3
DH = 128
WIN1 = 128
WIN2 = 512
WIN3 = 2048
SECOND_DILATION = 4
THIRD_DILATION = 16


ROPE_BASE = 500000.0

LAYERS = 4


def from_behind(block, axis, distance):
    devices = range(lax.axis_size(axis))
    route = [(i - distance, i) for i in devices if i - distance in devices]
    return lax.ppermute(block, axis, route)


def rotate(projected, offset):
    tok_rows = projected.shape[0]
    head_size = projected.shape[-1]
    half_size = head_size // 2
    positions = (offset + jnp.arange(tok_rows, dtype=jnp.int32)).astype(jnp.float32)
    frequency = 1.0 / ROPE_BASE ** (jnp.arange(0, head_size, 2, dtype=jnp.float32) / head_size)
    angles = (positions[:, None] * frequency[None, :]).reshape(tok_rows, 1, 1, half_size)
    cosine = jnp.cos(angles)
    sine_part = jnp.sin(angles)
    first_half = projected[..., :half_size]
    second_half = projected[..., half_size:]
    return jnp.concatenate(
        [
            first_half * cosine - second_half * sine_part,
            second_half * cosine + first_half * sine_part,
        ],
        axis=-1,
    )


def window_attend(query_part, buffer, steps, stride, offset):
    tok_rows, heads_here, head_size = query_part.shape
    sub_rows = tok_rows // stride
    key_rows = buffer.shape[1] // stride
    query_sub = query_part.reshape(sub_rows, stride, heads_here, head_size).transpose(1, 2, 0, 3)
    pair_sub = buffer.reshape(2, key_rows, stride, heads_here, head_size).transpose(0, 2, 3, 1, 4)
    block_rows = math.gcd(sub_rows, steps) if sub_rows > steps else sub_rows
    block_list = sub_rows // block_rows
    query_blocks = query_sub.reshape(stride, heads_here, block_list, block_rows, head_size)
    key_blocks = jnp.stack(
        [
            pair_sub[:, :, :, index * block_rows : index * block_rows + block_rows + steps]
            for index in range(block_list)
        ],
        axis=3,
    )
    scores = jnp.einsum(
        "zhnqe,zhnke->zhnqk", query_blocks, key_blocks[0], preferred_element_type=jnp.float32
    ) * head_size ** (-0.5)
    query_index = (jnp.arange(block_list, dtype=jnp.int32) * block_rows)[
        :, None, None
    ] + jnp.arange(block_rows, dtype=jnp.int32)[None, :, None]
    key_index = (jnp.arange(block_list, dtype=jnp.int32) * block_rows)[:, None, None] + jnp.arange(
        block_rows + steps, dtype=jnp.int32
    )[None, None, :]
    spacing = query_index + steps - key_index
    residue = jnp.arange(stride, dtype=jnp.int32)[:, None, None, None]
    key_position = offset + (key_index[None] - steps) * stride + residue
    allowed = (spacing[None] >= 0) & (spacing[None] <= steps) & (key_position >= 0)
    scores = jnp.where(allowed[:, None], scores, -jnp.inf)
    row_max = jnp.max(scores, axis=-1)
    exponent = jnp.exp(scores - row_max[..., None])
    totals = jnp.sum(exponent, axis=-1)
    probs = (exponent / totals[..., None]).astype(jnp.bfloat16)
    mixed = jnp.einsum(
        "zhnqk,zhnke->zhnqe", probs, key_blocks[1], preferred_element_type=jnp.float32
    )
    mixed = mixed.reshape(stride, heads_here, sub_rows, head_size).transpose(2, 0, 1, 3)
    log_total = (row_max + jnp.log(totals)).reshape(stride, heads_here, sub_rows).transpose(2, 0, 1)
    return (mixed.reshape(tok_rows, heads_here, head_size), log_total.reshape(tok_rows, heads_here))


def reach_back(key_value, distance_max):
    tok_rows = key_value.shape[1]
    gathered = key_value
    pieces_held = 1
    while pieces_held < distance_max + 1:
        slice_share = min(pieces_held, distance_max + 1 - pieces_held)
        arrived = from_behind(
            gathered[:, gathered.shape[1] - slice_share * tok_rows :], "sp", pieces_held
        )
        gathered = jnp.concatenate([arrived, gathered], axis=1)
        pieces_held = pieces_held + slice_share
    return gathered


def on_device(tokens, w_query, w_key, w_value, w_out):
    tok_rows = tokens.shape[0]
    heads_here = w_out.shape[0] // DH
    offset = lax.axis_index("sp") * tok_rows
    weight_parts = (
        lax.all_gather(w_query, "sp", axis=0, tiled=True),
        lax.all_gather(w_key, "sp", axis=0, tiled=True),
        lax.all_gather(w_value, "sp", axis=0, tiled=True),
    )
    query_raw, key_raw, value_raw = tuple(
        (
            jnp.dot(tokens, weight_rows, preferred_element_type=jnp.float32)
            for weight_rows in weight_parts
        )
    )
    head_shape = (tok_rows, heads_here, GROUPS, DH)
    queries = rotate(query_raw.reshape(head_shape), offset).astype(jnp.bfloat16)
    keys_all = rotate(key_raw.reshape(head_shape), offset).astype(jnp.bfloat16)
    values_all = value_raw.astype(jnp.bfloat16).reshape(head_shape)
    windows = (WIN1, WIN2, WIN3)
    step_sizes = (1, SECOND_DILATION, THIRD_DILATION)
    outputs = []
    log_totals = []
    for group_index in range(GROUPS):
        key_value = jnp.stack([keys_all[:, :, group_index], values_all[:, :, group_index]])
        key_value = key_value.reshape(2, tok_rows, heads_here * DH)
        window = windows[group_index]
        if group_index == 0:
            near_rows = from_behind(key_value[:, tok_rows - window :], "sp", 1)
            buffer = jnp.concatenate([near_rows, key_value], axis=1)
        else:
            distance_max = (window + tok_rows - 1) // tok_rows
            buffer = reach_back(key_value, distance_max)
        group_out, log_total = window_attend(
            queries[:, :, group_index],
            buffer,
            window // step_sizes[group_index],
            step_sizes[group_index],
            offset,
        )
        outputs.append(group_out)
        log_totals.append(log_total)
    group_weights = jax.nn.softmax(jnp.stack(log_totals), axis=0)
    merged = jnp.sum(group_weights[..., None] * jnp.stack(outputs), axis=0).astype(jnp.bfloat16)
    merged = merged.reshape(tok_rows, heads_here * DH)
    w_whole = lax.all_gather(w_out, "sp", axis=1, tiled=True)
    return lax.psum_scatter(
        jnp.dot(merged, w_whole, preferred_element_type=jnp.float32).astype(jnp.bfloat16),
        "tp",
        scatter_dimension=0,
        tiled=True,
    )


def layer_kernel(
    nz,
    tokens, w_key, w_value, w_query, w_out, out,
    weights, stage, tok_in, tok_turned, cosine, sine, queries, pair0, near_own, near_in, far2,
    out_rows, mine, heads_in, got01, top01, sum01,
    stage_s, swap_s, tok_r, w_r, up_s, down_s, side_s, o_r, o_s, o_r2, far_s, far_r, near_s, near_r, head_s, head_r,
):
    tok_rows, depth = tokens.shape
    k_rows, cols = w_key.shape
    sub = tok_rows // THIRD_DILATION
    sub_log = sub.bit_length() - 1
    block = tok_rows // SECOND_DILATION
    tail = WIN1
    last = nz - 1
    sp, tp = lax.axis_index("sp"), lax.axis_index("tp")
    z, y = sp // 2, sp % 2
    x, c = tp // 2, tp % 2
    rank = 2 * z + c
    stays = c == y
    moves = jnp.logical_not(stays)
    has_up, has_down = z < last, z > 0
    side = (sp, 2 * x + 1 - c)
    across_x = (sp, 2 * (1 - x) + c)
    across_y = (2 * z + 1 - y, tp)
    partner = (2 * z + 1 - y, 2 * x + 1 - c)
    above, below = (sp + 2, tp), (sp - 2, tp)
    up_other = (sp + 2, 2 * x)

    def send(src, dst, s_sem, r_sem, where):
        return pltpu.make_async_remote_copy(
            src_ref=src, dst_ref=dst, send_sem=s_sem, recv_sem=r_sem,
            device_id=where, device_id_type=pl.DeviceIdType.MESH,
        )

    parts = (w_key, w_value, w_query)
    upward, downward = (2, 0, 1), (0, 1, 2)

    def chunk(a, s):
        return weights.at[a, pl.ds(pl.multiple_of(s * k_rows, k_rows), k_rows), :]

    def o_chunk(zz):
        return out_rows.at[c, y, x, zz]

    def kept(a):
        return pltpu.make_async_copy(parts[a], chunk(a, rank), w_r.at[a, rank])

    def staged(a):
        return pltpu.make_async_copy(parts[a], stage.at[a], stage_s.at[a])

    def swapped(a):
        there = 2 * z + 1 - c
        return send(stage.at[a], chunk(a, there), swap_s.at[a], w_r.at[a, there], partner)

    def tok_kept():
        return pltpu.make_async_copy(tokens, tok_in, tok_r)

    def tok_swapped():
        return send(tokens, tok_in, swap_s.at[3], tok_r, partner)

    def o_kept():
        return pltpu.make_async_copy(w_out, o_chunk(z), o_r.at[z])

    o_kept().start()

    @pl.when(stays)
    def _():
        for a in (2, 0, 1):
            kept(a).start()
        tok_kept().start()

    @pl.when(moves)
    def _():
        for a in (2, 0, 1):
            staged(a).start()

    barrier = pltpu.get_barrier_semaphore()

    def greet(where):
        pl.semaphore_signal(barrier, inc=1, device_id=where, device_id_type=pl.DeviceIdType.MESH)

    for dy in range(2):
        for dx in range(2):
            for dc in range(2):
                if dy + dx + dc:
                    greet((2 * z + (y + dy) % 2, 2 * ((x + dx) % 2) + (c + dc) % 2))
    pl.when(has_up)(lambda: greet(above))
    pl.when(has_down)(lambda: greet(below))
    pl.when(has_up & (c == 1))(lambda: greet(up_other))
    pl.when(has_down & (c == 0))(lambda: greet((sp - 2, 2 * x + 1)))
    pl.semaphore_wait(barrier, 7 + jnp.where(has_up, 1 + c, 0) + jnp.where(has_down, 2 - c, 0))

    def go(a, zz, kind):
        s = 2 * zz + c
        ref = chunk(a, s) if a < 3 else o_chunk(zz)
        r_sem = w_r.at[a, s] if a < 3 else o_r.at[zz]
        s_sem = {"up": up_s, "down": down_s, "side": side_s}[kind].at[a, zz]
        return send(ref, ref, s_sem, r_sem, {"up": above, "down": below, "side": side}[kind])

    def swap_order(layer):
        return {0: (2, 0, 1), last: (0, 1, 2)}.get(layer, (0, 2, 1))

    @pl.when(moves)
    def _():
        for layer in range(nz):
            @pl.when(z == layer)
            def _(layer=layer):
                for a in swap_order(layer):
                    staged(a).wait()
                    swapped(a).start()
        tok_swapped().start()

    def o_relay(layer, d):
        if layer - d >= 0:
            go(3, layer - d, "up").wait_recv()
            if layer < last:
                go(3, layer - d, "up").start()
        if layer + d < nz:
            go(3, layer + d, "down").wait_recv()
            if layer > 0:
                go(3, layer + d, "down").start()

    def o_share(axis):
        ref, where = (
            (out_rows.at[c, y, x], across_x),
            (out_rows.at[c, y], across_y),
            (out_rows.at[c], side),
        )[axis]
        return send(ref, ref, o_s.at[axis], o_r2.at[axis], where)

    def events(layer):
        listed = []
        for i in range(3):
            for d in range(1, layer + 1):
                listed.append((i * layer + d, "up", upward[i], layer - d, d))
            for d in range(1, last - layer + 1):
                listed.append((i * (last - layer) + d, "down", downward[i], layer + d, d))
        return sorted(listed)

    def handle(layer, event):
        _, kind, a, zz, d = event
        go(a, zz, kind).wait_recv()
        if kind == "up":
            if layer < last:
                go(a, zz, "up").start()
            if d == layer and a == upward[0] and layer < last:
                go(upward[2], layer, "up").start()
        else:
            if layer > 0:
                go(a, zz, "down").start()
            if d == last - layer and a == downward[0] and layer > 0:
                go(downward[2], layer, "down").start()
        go(a, zz, "side").start()

    def begin(layer):
        o_kept().wait()
        if layer < last:
            go(3, layer, "up").start()
        if layer > 0:
            go(3, layer, "down").start()
        for a in swap_order(layer):
            pl.when(stays)(lambda a=a: kept(a).wait())
            pl.when(moves)(lambda a=a: go(a, layer, "side").wait_recv())
            if layer < last and (layer == 0 or a != upward[2]):
                go(a, layer, "up").start()
            if layer > 0 and (layer == last or a != downward[2]):
                go(a, layer, "down").start()
            go(a, layer, "side").start()

    def row_time(p):
        b, i = p >> sub_log, p & (sub - 1)
        return THIRD_DILATION * i + (b >> 2) + SECOND_DILATION * (b & 3)

    def tail_time(u):
        per = tail // THIRD_DILATION
        b, i = u >> (per.bit_length() - 1), u & (per - 1)
        return THIRD_DILATION * (sub - per + i) + (b >> 2) + SECOND_DILATION * (b & 3) - tok_rows

    def iota(shape, axis):
        return lax.broadcasted_iota(jnp.int32, shape, axis)

    def angles(index, carry):
        at = index * block
        rows = pl.ds(pl.multiple_of(at, block), block)
        pair_at = iota((1, DH), 1) & (DH // 2 - 1)
        freq = jnp.exp(pair_at.astype(jnp.float32) * (-2.0 * math.log(ROPE_BASE) / DH))
        angle = (row_time(iota((block, DH), 0) + at) + rank * tok_rows).astype(jnp.float32) * freq
        cosine[rows, :] = jnp.cos(angle)
        turned = jnp.sin(angle)
        sine[rows, :] = jnp.where(iota((block, DH), 1) < DH // 2, -turned, turned)
        return carry

    def order():
        p = row_time(iota((tok_rows, tok_rows), 0))
        t = iota((tok_rows, tok_rows), 1)
        pick = jnp.where(p == t, 1.0, 0.0).astype(jnp.bfloat16)

        def piece(index, carry):
            at = pl.ds(pl.multiple_of(index * 256, 256), 256)
            tok_turned[:, at] = jnp.dot(
                pick, tok_in[:, at], preferred_element_type=jnp.float32
            ).astype(jnp.bfloat16)
            return carry

        lax.fori_loop(0, depth // 256, piece, 0)

    def project(a, store):
        def piece(index, carry):
            rows = pl.ds(pl.multiple_of(index * block, block), block)
            raw = jnp.dot(tok_turned[rows, :], weights[a], preferred_element_type=jnp.float32)
            for g in range(GROUPS):
                part = raw[:, g * DH : (g + 1) * DH]
                if a != 1:
                    part = part * cosine[rows, :] + pltpu.roll(part, DH // 2, 1) * sine[rows, :]
                store(index, rows, g, part)
            return carry

        lax.fori_loop(0, SECOND_DILATION, piece, 0)

    def keep_pair(which):
        def store(index, rows, g, part):
            if g == 2:
                far2[4 + c, which, rows, :] = part.astype(jnp.bfloat16)
            elif g == 1:
                near_own[which, rows, :] = part.astype(jnp.bfloat16)
            else:
                pair0[which, rows, :] = part.astype(jnp.bfloat16)
                per = tail // THIRD_DILATION
                ends = jnp.concatenate(
                    [part[b * sub + sub - per : (b + 1) * sub] for b in range(4)], axis=0
                )
                at = pl.ds(pl.multiple_of(tok_rows + index * 4 * per, 4 * per), 4 * per)
                near_own[which, at, :] = ends.astype(jnp.bfloat16)

        return store

    def keep_query(index, rows, g, part):
        queries[g, rows, :] = part.astype(jnp.bfloat16)

    def others(a):
        for zz in range(nz):
            s = 2 * zz + 1 - c
            send(chunk(a, s), chunk(a, s), side_s.at[a, zz], w_r.at[a, s], side).wait_recv()

    def far(kind, src, dst, where):
        return send(far2.at[src], far2.at[dst], far_s.at[kind], far_r.at[dst], where)

    def own_side():
        return far(0, 4 + c, 4 + c, side)

    def own_up():
        return far(1, 4 + c, 2 + c, above)

    def pass_side(kind, slot):
        return far(kind, slot, slot, side)

    def pass_up():
        return far(3, 2 + c, c, above)

    def near(where):
        return send(near_own, near_in, near_s, near_r, where)

    def halos():
        pl.when(has_up & (c == 1))(lambda: near(up_other).start())
        pl.when(has_up)(lambda: own_up().start())
        pl.when(c == 0)(lambda: near(side).start())
        pl.when(c == 0)(lambda: own_side().start())

    scale = DH ** (-0.5)
    far_off = 1 << 24

    def dots(q, k):
        return lax.dot_general(q, k, (((1,), (1,)), ((), ())), preferred_element_type=jnp.float32)

    def soft(scores, time_q, time_k, reach, first):
        gap = time_q - jnp.where(time_k >= first, time_k, far_off)
        scores = jnp.where((gap >= 0) & (gap <= reach), scores * scale, -jnp.inf)
        top = jnp.max(scores, axis=-1, keepdims=True)
        weight = jnp.exp(scores - top)
        return top, jnp.sum(weight, axis=-1, keepdims=True), weight.astype(jnp.bfloat16)

    def near_groups():
        def piece(index, carry):
            begin = index * block
            rows = pl.ds(pl.multiple_of(begin, block), block)
            q = queries[0, rows, :]
            tails = pl.ds(tok_rows, tail)
            scores = jnp.concatenate([dots(q, near_in[0, tails, :]), dots(q, pair0[0])], axis=1)
            lane = iota((1, tail + tok_rows), 1)
            time_k = jnp.where(lane < tail, tail_time(lane & (tail - 1)), row_time(lane - tail))
            time_q = row_time(iota((block, 1), 0) + begin)
            top0, sum0, weight = soft(scores, time_q, time_k, WIN1, -rank * tok_rows)
            got0 = jnp.dot(weight[:, :tail], near_in[1, tails, :], preferred_element_type=jnp.float32)
            got0 += jnp.dot(weight[:, tail:], pair0[1], preferred_element_type=jnp.float32)
            q = queries[1, rows, :]
            scores = jnp.concatenate(
                [dots(q, near_in[0, rows, :]), dots(q, near_own[0, rows, :])], axis=1
            )

            def step_of(place):
                return 4 * (place & (sub - 1)) + (place >> sub_log)

            lane = iota((1, 2 * block), 1)
            step_k = step_of(lane & (block - 1)) + jnp.where(lane < block, -block, 0)
            top1, sum1, weight = soft(
                scores, step_of(iota((block, 1), 0)), step_k, WIN2 // SECOND_DILATION, -rank * block
            )
            got1 = jnp.dot(weight[:, :block], near_in[1, rows, :], preferred_element_type=jnp.float32)
            got1 += jnp.dot(weight[:, block:], near_own[1, rows, :], preferred_element_type=jnp.float32)
            top = jnp.maximum(top0, top1)
            f0, f1 = jnp.exp(top0 - top), jnp.exp(top1 - top)
            got01[rows, :] = f0 * got0 + f1 * got1
            top01[rows, :] = top
            sum01[rows, :] = f0 * sum0 + f1 * sum1
            return carry

        lax.fori_loop(0, SECOND_DILATION, piece, 0)

    def far_group():
        slots = [4 + c - d for d in (4, 3, 2, 1, 0)]

        def piece(index, carry):
            begin = index * block
            rows = pl.ds(pl.multiple_of(begin, block), block)
            all_scores = []
            for b in range(4):
                here = pl.ds(pl.multiple_of(begin + b * sub, sub), sub)
                keys = jnp.concatenate([far2[s, 0, here, :] for s in slots], axis=0)
                all_scores.append(dots(queries[2, here, :], keys))
            scores = jnp.concatenate(all_scores, axis=0)
            step_q = iota((block, 1), 0) & (sub - 1)
            step_k = iota((1, 5 * sub), 1) - 4 * sub
            top2, sum2, weight = soft(scores, step_q, step_k, WIN3 // THIRD_DILATION, -rank * sub)
            got = []
            for b in range(4):
                here = pl.ds(pl.multiple_of(begin + b * sub, sub), sub)
                vals = jnp.concatenate([far2[s, 1, here, :] for s in slots], axis=0)
                got.append(
                    jnp.dot(weight[b * sub : (b + 1) * sub], vals, preferred_element_type=jnp.float32)
                )
            got2 = jnp.concatenate(got, axis=0)
            top1 = top01[rows, :]
            top = jnp.maximum(top1, top2)
            f1, f2 = jnp.exp(top1 - top), jnp.exp(top2 - top)
            total = f1 * sum01[rows, :] + f2 * sum2
            mine[0, rows, :] = ((f1 * got01[rows, :] + f2 * got2) / total).astype(jnp.bfloat16)
            return carry

        lax.fori_loop(0, SECOND_DILATION, piece, 0)
        t = iota((tok_rows, tok_rows), 0)
        p = row_time(iota((tok_rows, tok_rows), 1))
        mine[1] = jnp.dot(
            jnp.where(p == t, 1.0, 0.0).astype(jnp.bfloat16), mine[0], preferred_element_type=jnp.float32
        ).astype(jnp.bfloat16)

    head = 2 * x + y
    quarter = tok_rows // 4

    def deal(k):
        return send(
            mine.at[1, pl.ds(k * quarter, quarter), :], heads_in.at[head], head_s.at[k], head_r.at[head], (rank, k)
        )

    def deal_self(k):
        return pltpu.make_async_copy(mine.at[1, pl.ds(k * quarter, quarter), :], heads_in.at[head], head_r.at[head])

    def turn_tokens():
        pl.when(stays)(lambda: tok_kept().wait())
        pl.when(moves)(lambda: tok_swapped().wait_recv())
        order()

    def key_value(which):
        others(which)
        project(which, keep_pair(which))

    def query():
        others(2)
        project(2, keep_query)

    def run(layer):
        begin(layer)
        o_relay(layer, 1)
        lax.fori_loop(0, SECOND_DILATION, angles, 0)
        pl.when(stays)(turn_tokens)
        todo = events(layer)
        for event in todo[:3]:
            handle(layer, event)
        o_relay(layer, 2)
        o_relay(layer, 3)
        o_share(0).start()
        split = 9 if layer == 2 else 6 if layer != 1 else 7
        for event in todo[3:split]:
            handle(layer, event)
        late = todo[split:]
        if layer == 1:
            @pl.when(moves)
            def _():
                for event in late:
                    handle(layer, event)

        o_share(0).wait()
        o_share(1).start()
        pl.when(moves)(turn_tokens)
        if layer == last:
            query()
            key_value(0)
        else:
            key_value(0)
            key_value(1)
            halos()
        if layer == 1:
            @pl.when(stays)
            def _():
                for event in late:
                    handle(layer, event)
        else:
            for event in late:
                handle(layer, event)
        if layer == last:
            key_value(1)
            halos()
        else:
            query()

    for layer in range(nz):
        pl.when(z == layer)(functools.partial(run, layer))

    for slot in range(4):
        @pl.when(2 * z + slot < 4)
        def _(slot=slot):
            far2[slot] = jnp.zeros(far2.shape[1:], far2.dtype)

    @pl.when(rank == 0)
    def _():
        near_in[...] = jnp.zeros(near_in.shape, near_in.dtype)

    pl.when(rank >= 1)(lambda: near(side).wait_recv())
    near_groups()
    o_share(1).wait()
    o_share(2).start()

    @pl.when(z >= 1)
    def _():
        own_up().wait_recv()
        pl.when(has_up)(lambda: pass_up().start())
        pass_side(2, 2 + c).start()

    @pl.when(z >= 2)
    def _():
        pass_up().wait_recv()
        pl.when(c == 1)(lambda: pass_side(4, 1).start())
        pl.when(c == 0)(lambda: pass_side(4, 1).wait_recv())

    pl.when(c == 1)(lambda: pass_side(0, 4).wait_recv())
    pl.when(z >= 1)(lambda: pass_side(2, 3 - c).wait_recv())
    far_group()
    for k in range(4):
        self_here = stays & (tp == k)
        pl.when(self_here)(lambda k=k: deal_self(k).start())
        pl.when(jnp.logical_not(self_here))(lambda k=k: deal(k).start())

    o_share(2).wait()
    for h in range(4):
        pltpu.make_async_copy(heads_in.at[h], heads_in.at[h], head_r.at[h]).wait()
    for zz in range(nz):
        for yy in range(2):
            acc = None
            for h in range(4):
                one = jnp.dot(heads_in[h], out_rows[h % 2, yy, h // 2, zz], preferred_element_type=jnp.float32)
                acc = one if acc is None else acc + one
            width = w_out.shape[1]
            s = 2 * zz + yy
            out[:, s * width : (s + 1) * width] = acc.astype(jnp.bfloat16)

    for k in range(4):
        pl.when(jnp.logical_not(stays & (tp == k)))(lambda k=k: deal(k).wait_send())

    @pl.when(moves)
    def _():
        for a in range(3):
            swapped(a).wait_send()
        tok_swapped().wait_send()

    for a in range(4):
        for zz in range(nz):
            pl.when(has_up & (zz <= z))(lambda a=a, zz=zz: go(a, zz, "up").wait_send())
            pl.when(has_down & (zz >= z))(lambda a=a, zz=zz: go(a, zz, "down").wait_send())
            if a < 3:
                go(a, zz, "side").wait_send()
    pl.when((c == 0) | has_up)(lambda: near(side).wait_send())
    pl.when(c == 0)(lambda: own_side().wait_send())
    pl.when(has_up)(lambda: own_up().wait_send())
    pl.when(z >= 1)(lambda: pass_side(2, 2 + c).wait_send())
    pl.when((z >= 1) & has_up)(lambda: pass_up().wait_send())
    pl.when((z >= 2) & (c == 1))(lambda: pass_side(4, 1).wait_send())


def fits_kernel(n_sp, n_tp, tokens, w_query, w_out):
    tok_rows, depth = tokens.shape
    return (
        n_sp == 2 * LAYERS
        and n_tp == 4
        and w_query.shape[1] == GROUPS * DH
        and w_out.shape[0] == DH
        and w_out.shape[1] % 128 == 0
        and w_query.shape[0] % 16 == 0
        and tok_rows == WIN2
        and 4 * tok_rows == WIN3
        and 4 * WIN1 == tok_rows
    )


def one_kernel(n_sp, tokens, w_query, w_key, w_value, w_out):
    nz = n_sp // 2
    tok_rows, depth = tokens.shape
    cols = w_query.shape[1]
    bf, dma = jnp.bfloat16, pltpu.SemaphoreType.DMA
    return pl.pallas_call(
        functools.partial(layer_kernel, nz),
        out_shape=jax.ShapeDtypeStruct((tok_rows // 4, w_out.shape[1] * n_sp), bf),
        in_specs=[pl.BlockSpec(memory_space=pltpu.HBM)] * 5,
        out_specs=pl.BlockSpec(memory_space=pltpu.VMEM),
        scratch_shapes=[
            pltpu.VMEM((3, depth, cols), bf),
            pltpu.VMEM((3, *w_query.shape), bf),
            pltpu.VMEM((tok_rows, depth), bf),
            pltpu.VMEM((tok_rows, depth), bf),
            pltpu.VMEM((tok_rows, DH), jnp.float32),
            pltpu.VMEM((tok_rows, DH), jnp.float32),
            pltpu.VMEM((GROUPS, tok_rows, DH), bf),
            pltpu.VMEM((2, tok_rows, DH), bf),
            pltpu.VMEM((2, tok_rows + WIN1, DH), bf),
            pltpu.VMEM((2, tok_rows + WIN1, DH), bf),
            pltpu.VMEM((6, 2, tok_rows, DH), bf),
            pltpu.VMEM((2, 2, 2, nz, *w_out.shape), bf),
            pltpu.VMEM((2, tok_rows, DH), bf),
            pltpu.VMEM((4, tok_rows // 4, DH), bf),
            pltpu.VMEM((tok_rows, DH), jnp.float32),
            pltpu.VMEM((tok_rows, 1), jnp.float32),
            pltpu.VMEM((tok_rows, 1), jnp.float32),
            dma((3,)), dma((4,)), dma, dma((3, n_sp)), dma((4, nz)), dma((4, nz)), dma((3, nz)),
            dma((nz,)), dma((3,)), dma((3,)),
            dma((5,)), dma((6,)), dma, dma, dma((4,)), dma((4,)),
        ],
        compiler_params=pltpu.CompilerParams(
            collective_id=0, has_side_effects=True, vmem_limit_bytes=60 * 1024 * 1024
        ),
    )(tokens, w_key, w_value, w_query, w_out)


def on_mesh(n_sp, n_tp, *operands):
    tokens, w_query, _, _, w_out = operands
    if fits_kernel(n_sp, n_tp, tokens, w_query, w_out):
        return one_kernel(n_sp, *operands)
    return on_device(*operands)


def solution(mesh):
    placed = (P("sp", None), P("sp", "tp"), P("sp", "tp"), P("sp", "tp"), P("tp", "sp"))
    body = functools.partial(on_mesh, mesh.shape["sp"], mesh.shape["tp"])
    return jax.shard_map(
        body, mesh=mesh, in_specs=placed, out_specs=P(("sp", "tp"), None), check_vma=False
    )
```

time: 78.9 us -> 73 us (0.925)
  Pallas kernels: 76.8 us -> 71 us
    pallas_call x1, Pallas kernels: 76.8 us -> 71 us  [one_kernel(): pl.pallas_call(functools.partial(layer_kernel, nz), out_shape=jax.ShapeDt...]
where the time goes in v2:
time: 73 us; the launch traced here: 72.9 us
  Pallas kernels  71 us (97%)
  local copies, waits for them, and re-layouts  1.88 us (3%)
    pallas_call x1, Pallas kernels, one_kernel(): pl.pallas_call(functools.partial(layer_kernel, nz), out_shape=jax.ShapeDt...  71 us
    unnamed x1, local copies, waits for them, and re-layouts  1.88 us

profile of v2, /device:TPU:25, one launch (start us, length us, event | category | flops | bytes accessed | tf_op | source)
XLA Modules:
  0.0 72.9 jit_solution(1053978388135387683)
XLA Ops:
  0.0 71.0 %shard_map.55 = bf16[128,2048]{1,0:T(8,128)(2,1)} custom-call(bf16[512,2048]{1,0:T(8,128)(2,1)} %tokens.1, bf16[256,384]{1,0:T(8,128)(2,1)} %w_key.1, bf16[256,384]{1,0:T(8,128)(2,1)} %w_value.1, bf16[256,384]{1,0:T(8,128)(2,1)} %w_query.1, bf16[128,256]{1,0:T(8,128)(2,1)} %w_out.1), custom_call_target="tpu_custom_call" | custom-call | tf_op jit(solution)/shard_map/pallas_call | solution.py:677
  71.0 1.9 %copy.7 = bf16[128,2048]{1,0:T(8,128)(2,1)} copy(bf16[128,2048]{1,0:T(8,128)(2,1)} %shard_map.55) | data formatting | bytes 1048576

commit v3 on v2

--- a/solution.py
+++ b/solution.py
@@ -162,8 +162,8 @@
     nz,
     tokens, w_key, w_value, w_query, w_out, out,
     weights, stage, tok_in, tok_turned, cosine, sine, queries, pair0, near_own, near_in, far2,
-    out_rows, mine, heads_in, got01, top01, sum01,
-    stage_s, swap_s, tok_r, w_r, up_s, down_s, side_s, o_r, o_s, o_r2, far_s, far_r, near_s, near_r, head_s, head_r,
+    out_rows, mine, heads_in, got01, top01, sum01, asked, part, part_log, got_part, got_log,
+    stage_s, swap_s, tok_k, t_r, ty_s, tx_s, w_r, up_s, down_s, side_s, o_r, o_s, o_r2, far_s, far_r, near_s, near_r, head_s, head_r, part_s, part_r,
 ):
     tok_rows, depth = tokens.shape
     k_rows, cols = w_key.shape
@@ -212,10 +212,25 @@
         return send(stage.at[a], chunk(a, there), swap_s.at[a], w_r.at[a, there], partner)
 
     def tok_kept():
-        return pltpu.make_async_copy(tokens, tok_in, tok_r)
-
-    def tok_swapped():
-        return send(tokens, tok_in, swap_s.at[3], tok_r, partner)
+        return pltpu.make_async_copy(tokens, tok_in, tok_k)
+
+    pieces = ty_s.shape[0]
+    piece_rows = tok_rows // 2 // pieces
+
+    def piece_at(half, q):
+        return pl.ds(pl.multiple_of(half * (tok_rows // 2) + q * piece_rows, piece_rows), piece_rows)
+
+    def t_y(q):
+        at = piece_at(x, q)
+        return send(tokens.at[at, :], tok_in.at[at, :], ty_s.at[q], t_r.at[x, q], partner)
+
+    def t_x(half, q):
+        at = piece_at(half, q)
+        return send(tok_in.at[at, :], tok_in.at[at, :], tx_s.at[q], t_r.at[half, q], across_x)
+
+    def pass_token(q):
+        t_y(q).wait_recv()
+        t_x(x, q).start()
 
     def o_kept():
         return pltpu.make_async_copy(w_out, o_chunk(z), o_r.at[z])
@@ -267,7 +282,8 @@
                 for a in swap_order(layer):
                     staged(a).wait()
                     swapped(a).start()
-        tok_swapped().start()
+        for q in range(pieces):
+            t_y(q).start()
 
     def o_relay(layer, d):
         if layer - d >= 0:
@@ -302,13 +318,11 @@
         if kind == "up":
             if layer < last:
                 go(a, zz, "up").start()
-            if d == layer and a == upward[0] and layer < last:
+            if d == layer and a == upward[1] and layer < last:
                 go(upward[2], layer, "up").start()
         else:
             if layer > 0:
                 go(a, zz, "down").start()
-            if d == last - layer and a == downward[0] and layer > 0:
-                go(downward[2], layer, "down").start()
         go(a, zz, "side").start()
 
     def begin(layer):
@@ -404,6 +418,9 @@
     def far(kind, src, dst, where):
         return send(far2.at[src], far2.at[dst], far_s.at[kind], far_r.at[dst], where)
 
+    gives_up, takes_up = z < last - 1, (z > 0) & (z < last)
+    helps, asks = z == last - 1, z == last
+
     def own_side():
         return far(0, 4 + c, 4 + c, side)
 
@@ -420,10 +437,19 @@
         return send(near_own, near_in, near_s, near_r, where)
 
     def halos():
+        pl.when(gives_up)(lambda: own_up().start())
         pl.when(has_up & (c == 1))(lambda: near(up_other).start())
-        pl.when(has_up)(lambda: own_up().start())
         pl.when(c == 0)(lambda: near(side).start())
-        pl.when(c == 0)(lambda: own_side().start())
+        pl.when((c == 0) | helps)(lambda: own_side().start())
+
+    def ask():
+        return send(queries.at[2], asked, part_s.at[0], part_r.at[0], below)
+
+    def answer():
+        return send(part, got_part, part_s.at[1], part_r.at[1], above)
+
+    def answer_log():
+        return send(part_log, got_log, part_s.at[2], part_r.at[2], above)
 
     scale = DH ** (-0.5)
     far_off = 1 << 24
@@ -475,37 +501,79 @@
 
         lax.fori_loop(0, SECOND_DILATION, piece, 0)
 
-    def far_group():
+    def far_piece(index, source, slots, reach_back, first, until=None):
+        begin = index * block
+
+        def rows_of(b):
+            return pl.ds(pl.multiple_of(begin + b * sub, sub), sub)
+
+        all_scores = []
+        for b in range(4):
+            keys = jnp.concatenate([far2[slot, 0, rows_of(b), :] for slot in slots], axis=0)
+            all_scores.append(dots(source[rows_of(b), :], keys))
+        scores = jnp.concatenate(all_scores, axis=0)
+        step_q = iota((block, 1), 0) & (sub - 1)
+        step_k = iota((1, len(slots) * sub), 1) - reach_back * sub
+        seen = step_k if until is None else jnp.where(step_k < until, step_k, far_off)
+        top, total, weight = soft(scores, step_q, seen, WIN3 // THIRD_DILATION, first)
+        got = []
+        for b in range(4):
+            vals = jnp.concatenate([far2[slot, 1, rows_of(b), :] for slot in slots], axis=0)
+            got.append(
+                jnp.dot(weight[b * sub : (b + 1) * sub], vals, preferred_element_type=jnp.float32)
+            )
+        return top, total, jnp.concatenate(got, axis=0)
+
+    def eye():
+        return iota((block, block), 0) == iota((block, block), 1)
+
+    def block_rows(index):
+        return pl.ds(pl.multiple_of(index * block, block), block)
+
+    def help_above():
+        slots = [2 + c, 3 + c, 4 + c, 5]
+
+        def piece(index, carry):
+            top, total, got = far_piece(index, asked, slots, 4, -4 * sub, -c * sub)
+            part[block_rows(index), :] = (got / total).astype(jnp.bfloat16)
+            row = jnp.sum(jnp.where(eye(), top + jnp.log(total), 0.0), axis=0, keepdims=True)
+            part_log[index] = jnp.broadcast_to(row, part_log.shape[1:])
+            return carry
+
+        lax.fori_loop(0, SECOND_DILATION, piece, 0)
+
+    def settle(rows, top2, sum2, got2):
+        top1 = top01[rows, :]
+        top = jnp.maximum(top1, top2)
+        f1, f2 = jnp.exp(top1 - top), jnp.exp(top2 - top)
+        total = f1 * sum01[rows, :] + f2 * sum2
+        mine[0, rows, :] = ((f1 * got01[rows, :] + f2 * got2) / total).astype(jnp.bfloat16)
+
+    def far_here():
         slots = [4 + c - d for d in (4, 3, 2, 1, 0)]
 
         def piece(index, carry):
-            begin = index * block
-            rows = pl.ds(pl.multiple_of(begin, block), block)
-            all_scores = []
-            for b in range(4):
-                here = pl.ds(pl.multiple_of(begin + b * sub, sub), sub)
-                keys = jnp.concatenate([far2[s, 0, here, :] for s in slots], axis=0)
-                all_scores.append(dots(queries[2, here, :], keys))
-            scores = jnp.concatenate(all_scores, axis=0)
-            step_q = iota((block, 1), 0) & (sub - 1)
-            step_k = iota((1, 5 * sub), 1) - 4 * sub
-            top2, sum2, weight = soft(scores, step_q, step_k, WIN3 // THIRD_DILATION, -rank * sub)
-            got = []
-            for b in range(4):
-                here = pl.ds(pl.multiple_of(begin + b * sub, sub), sub)
-                vals = jnp.concatenate([far2[s, 1, here, :] for s in slots], axis=0)
-                got.append(
-                    jnp.dot(weight[b * sub : (b + 1) * sub], vals, preferred_element_type=jnp.float32)
-                )
-            got2 = jnp.concatenate(got, axis=0)
-            top1 = top01[rows, :]
-            top = jnp.maximum(top1, top2)
-            f1, f2 = jnp.exp(top1 - top), jnp.exp(top2 - top)
-            total = f1 * sum01[rows, :] + f2 * sum2
-            mine[0, rows, :] = ((f1 * got01[rows, :] + f2 * got2) / total).astype(jnp.bfloat16)
+            settle(block_rows(index), *far_piece(index, queries.at[2], slots, 4, -rank * sub))
             return carry
 
         lax.fori_loop(0, SECOND_DILATION, piece, 0)
+
+    def far_asked():
+        slots = [3 + c, 4 + c]
+
+        def piece(index, carry):
+            rows = block_rows(index)
+            top_a, sum_a, got_a = far_piece(index, queries.at[2], slots, 1, -c * sub)
+            top_b = jnp.sum(jnp.where(eye(), got_log[index, 0:1, :], 0.0), axis=1, keepdims=True)
+            top2 = jnp.maximum(top_a, top_b)
+            fa, fb = jnp.exp(top_a - top2), jnp.exp(top_b - top2)
+            got2 = fa * got_a + fb * got_part[rows, :].astype(jnp.float32)
+            settle(rows, top2, fa * sum_a + fb, got2)
+            return carry
+
+        lax.fori_loop(0, SECOND_DILATION, piece, 0)
+
+    def unturn():
         t = iota((tok_rows, tok_rows), 0)
         p = row_time(iota((tok_rows, tok_rows), 1))
         mine[1] = jnp.dot(
@@ -525,7 +593,12 @@
 
     def turn_tokens():
         pl.when(stays)(lambda: tok_kept().wait())
-        pl.when(moves)(lambda: tok_swapped().wait_recv())
+
+        @pl.when(moves)
+        def _():
+            for q in range(pieces):
+                t_x(1 - x, q).wait_recv()
+
         order()
 
     def key_value(which):
@@ -535,6 +608,10 @@
     def query():
         others(2)
         project(2, keep_query)
+
+    def last_down(layer):
+        if 0 < layer < last:
+            go(downward[2], layer, "down").start()
 
     def run(layer):
         begin(layer)
@@ -542,34 +619,43 @@
         lax.fori_loop(0, SECOND_DILATION, angles, 0)
         pl.when(stays)(turn_tokens)
         todo = events(layer)
-        for event in todo[:3]:
-            handle(layer, event)
+        for q in range(3):
+            handle(layer, todo[q])
+            pl.when(moves)(lambda q=q: pass_token(q))
         o_relay(layer, 2)
-        o_relay(layer, 3)
-        o_share(0).start()
         split = 9 if layer == 2 else 6 if layer != 1 else 7
-        for event in todo[3:split]:
-            handle(layer, event)
+        downs = [i for i, event in enumerate(todo) if event[1:3] == ("down", downward[1])]
+        for i in range(3, split):
+            handle(layer, todo[i])
+            if i == 3:
+                pl.when(moves)(lambda: pass_token(3))
+            if layer == 2 and i == max(max(downs), 3):
+                last_down(layer)
         late = todo[split:]
         if layer == 1:
             @pl.when(moves)
             def _():
+                last_down(layer)
                 for event in late:
                     handle(layer, event)
 
-        o_share(0).wait()
-        o_share(1).start()
+        o_relay(layer, 3)
+        o_share(0).start()
         pl.when(moves)(turn_tokens)
         if layer == last:
             query()
+            ask().start()
             key_value(0)
         else:
             key_value(0)
             key_value(1)
             halos()
+        o_share(0).wait()
+        o_share(1).start()
         if layer == 1:
             @pl.when(stays)
             def _():
+                last_down(layer)
                 for event in late:
                     handle(layer, event)
         else:
@@ -585,34 +671,52 @@
         pl.when(z == layer)(functools.partial(run, layer))
 
     for slot in range(4):
-        @pl.when(2 * z + slot < 4)
+        @pl.when((2 * z + slot < 4) | (asks & (c == 0) & (slot == 3)))
         def _(slot=slot):
             far2[slot] = jnp.zeros(far2.shape[1:], far2.dtype)
 
     @pl.when(rank == 0)
     def _():
         near_in[...] = jnp.zeros(near_in.shape, near_in.dtype)
+
+    @pl.when(takes_up)
+    def _():
+        own_up().wait_recv()
+        pl.when(gives_up)(lambda: pass_up().start())
+        pass_side(2, 2 + c).start()
+
+    pl.when(c == 1)(lambda: pass_side(0, 4).wait_recv())
+
+    @pl.when(helps)
+    def _():
+        pl.when(c == 0)(lambda: pass_side(0, 5).wait_recv())
+        pass_side(2, 3 - c).wait_recv()
+        ask().wait_recv()
+        help_above()
+        answer().start()
+        answer_log().start()
 
     pl.when(rank >= 1)(lambda: near(side).wait_recv())
     near_groups()
     o_share(1).wait()
     o_share(2).start()
 
-    @pl.when(z >= 1)
-    def _():
-        own_up().wait_recv()
-        pl.when(has_up)(lambda: pass_up().start())
-        pass_side(2, 2 + c).start()
-
-    @pl.when(z >= 2)
+    @pl.when(helps)
     def _():
         pass_up().wait_recv()
         pl.when(c == 1)(lambda: pass_side(4, 1).start())
         pl.when(c == 0)(lambda: pass_side(4, 1).wait_recv())
 
-    pl.when(c == 1)(lambda: pass_side(0, 4).wait_recv())
-    pl.when(z >= 1)(lambda: pass_side(2, 3 - c).wait_recv())
-    far_group()
+    pl.when(takes_up & gives_up)(lambda: pass_side(2, 3 - c).wait_recv())
+
+    @pl.when(asks)
+    def _():
+        answer().wait_recv()
+        answer_log().wait_recv()
+        far_asked()
+
+    pl.when(jnp.logical_not(asks))(far_here)
+    unturn()
     for k in range(4):
         self_here = stays & (tp == k)
         pl.when(self_here)(lambda k=k: deal_self(k).start())
@@ -638,7 +742,9 @@
     def _():
         for a in range(3):
             swapped(a).wait_send()
-        tok_swapped().wait_send()
+        for q in range(pieces):
+            t_y(q).wait_send()
+            t_x(x, q).wait_send()
 
     for a in range(4):
         for zz in range(nz):
@@ -647,11 +753,17 @@
             if a < 3:
                 go(a, zz, "side").wait_send()
     pl.when((c == 0) | has_up)(lambda: near(side).wait_send())
-    pl.when(c == 0)(lambda: own_side().wait_send())
-    pl.when(has_up)(lambda: own_up().wait_send())
-    pl.when(z >= 1)(lambda: pass_side(2, 2 + c).wait_send())
-    pl.when((z >= 1) & has_up)(lambda: pass_up().wait_send())
-    pl.when((z >= 2) & (c == 1))(lambda: pass_side(4, 1).wait_send())
+    pl.when((c == 0) | helps)(lambda: own_side().wait_send())
+    pl.when(gives_up)(lambda: own_up().wait_send())
+    pl.when(takes_up)(lambda: pass_side(2, 2 + c).wait_send())
+    pl.when(takes_up & gives_up)(lambda: pass_up().wait_send())
+    pl.when(helps & (c == 1))(lambda: pass_side(4, 1).wait_send())
+    pl.when(asks)(lambda: ask().wait_send())
+
+    @pl.when(helps)
+    def _():
+        answer().wait_send()
+        answer_log().wait_send()
 
 
 def fits_kernel(n_sp, n_tp, tokens, w_query, w_out):
@@ -697,9 +809,14 @@
             pltpu.VMEM((tok_rows, DH), jnp.float32),
             pltpu.VMEM((tok_rows, 1), jnp.float32),
             pltpu.VMEM((tok_rows, 1), jnp.float32),
-            dma((3,)), dma((4,)), dma, dma((3, n_sp)), dma((4, nz)), dma((4, nz)), dma((3, nz)),
+            pltpu.VMEM((tok_rows, DH), bf),
+            pltpu.VMEM((tok_rows, DH), bf),
+            pltpu.VMEM((SECOND_DILATION, 8, DH), jnp.float32),
+            pltpu.VMEM((tok_rows, DH), bf),
+            pltpu.VMEM((SECOND_DILATION, 8, DH), jnp.float32),
+            dma((3,)), dma((3,)), dma, dma((2, 4)), dma((4,)), dma((4,)), dma((3, n_sp)), dma((4, nz)), dma((4, nz)), dma((3, nz)),
             dma((nz,)), dma((3,)), dma((3,)),
-            dma((5,)), dma((6,)), dma, dma, dma((4,)), dma((4,)),
+            dma((5,)), dma((6,)), dma, dma, dma((4,)), dma((4,)), dma((3,)), dma((3,)),
         ],
         compiler_params=pltpu.CompilerParams(
             collective_id=0, has_side_effects=True, vmem_limit_bytes=60 * 1024 * 1024

time: 73 us -> 68.1 us (0.933)
  the two profiles are of different devices: /device:TPU:25 before, /device:TPU:9 now
where the time goes in v3:
time: 68.1 us; the launch traced here: 67.9 us
  Pallas kernels  66.1 us (97%)
  local copies, waits for them, and re-layouts  1.88 us (3%)
    pallas_call x1, Pallas kernels, one_kernel(): pl.pallas_call(functools.partial(layer_kernel, nz), out_shape=jax.ShapeDt...  66.1 us
    unnamed x1, local copies, waits for them, and re-layouts  1.88 us

profile of v3, /device:TPU:9, one launch (start us, length us, event | category | flops | bytes accessed | tf_op | source)
XLA Modules:
  0.0 67.9 jit_solution(390232000064835475)
XLA Ops:
  0.0 66.1 %shard_map.55 = bf16[128,2048]{1,0:T(8,128)(2,1)} custom-call(bf16[512,2048]{1,0:T(8,128)(2,1)} %tokens.1, bf16[256,384]{1,0:T(8,128)(2,1)} %w_key.1, bf16[256,384]{1,0:T(8,128)(2,1)} %w_value.1, bf16[256,384]{1,0:T(8,128)(2,1)} %w_query.1, bf16[128,256]{1,0:T(8,128)(2,1)} %w_out.1), custom_call_target="tpu_custom_call" | custom-call | tf_op jit(solution)/shard_map/pallas_call | solution.py:789
  66.1 1.9 %copy.7 = bf16[128,2048]{1,0:T(8,128)(2,1)} copy(bf16[128,2048]{1,0:T(8,128)(2,1)} %shard_map.55) | data formatting | bytes 1048576

commit v4 on v3

--- a/solution.py
+++ b/solution.py
@@ -379,16 +379,18 @@
 
     def project(a, store):
         def piece(index, carry):
-            rows = pl.ds(pl.multiple_of(index * block, block), block)
-            raw = jnp.dot(tok_turned[rows, :], weights[a], preferred_element_type=jnp.float32)
-            for g in range(GROUPS):
-                part = raw[:, g * DH : (g + 1) * DH]
-                if a != 1:
-                    part = part * cosine[rows, :] + pltpu.roll(part, DH // 2, 1) * sine[rows, :]
-                store(index, rows, g, part)
+            both = pl.ds(pl.multiple_of(index * 2 * block, 2 * block), 2 * block)
+            whole = jnp.dot(tok_turned[both, :], weights[a], preferred_element_type=jnp.float32)
+            for k in range(2):
+                rows = pl.ds(pl.multiple_of((2 * index + k) * block, block), block)
+                for g in range(GROUPS):
+                    part = whole[k * block : (k + 1) * block, g * DH : (g + 1) * DH]
+                    if a != 1:
+                        part = part * cosine[rows, :] + pltpu.roll(part, DH // 2, 1) * sine[rows, :]
+                    store(2 * index + k, rows, g, part)
             return carry
 
-        lax.fori_loop(0, SECOND_DILATION, piece, 0)
+        lax.fori_loop(0, SECOND_DILATION // 2, piece, 0, unroll=2)
 
     def keep_pair(which):
         def store(index, rows, g, part):
@@ -499,7 +501,7 @@
             sum01[rows, :] = f0 * sum0 + f1 * sum1
             return carry
 
-        lax.fori_loop(0, SECOND_DILATION, piece, 0)
+        lax.fori_loop(0, SECOND_DILATION, piece, 0, unroll=4)
 
     def far_piece(index, source, slots, reach_back, first, until=None):
         begin = index * block
@@ -540,7 +542,7 @@
             part_log[index] = jnp.broadcast_to(row, part_log.shape[1:])
             return carry
 
-        lax.fori_loop(0, SECOND_DILATION, piece, 0)
+        lax.fori_loop(0, SECOND_DILATION, piece, 0, unroll=4)
 
     def settle(rows, top2, sum2, got2):
         top1 = top01[rows, :]
@@ -556,7 +558,7 @@
             settle(block_rows(index), *far_piece(index, queries.at[2], slots, 4, -rank * sub))
             return carry
 
-        lax.fori_loop(0, SECOND_DILATION, piece, 0)
+        lax.fori_loop(0, SECOND_DILATION, piece, 0, unroll=4)
 
     def far_asked():
         slots = [3 + c, 4 + c]
@@ -571,7 +573,7 @@
             settle(rows, top2, fa * sum_a + fb, got2)
             return carry
 
-        lax.fori_loop(0, SECOND_DILATION, piece, 0)
+        lax.fori_loop(0, SECOND_DILATION, piece, 0, unroll=4)
 
     def unturn():
         t = iota((tok_rows, tok_rows), 0)
@@ -613,59 +615,88 @@
         if 0 < layer < last:
             go(downward[2], layer, "down").start()
 
-    def run(layer):
+    def turn():
+        lax.fori_loop(0, SECOND_DILATION, angles, 0)
+        turn_tokens()
+
+    def moves_pass(q):
+        pl.when(moves)(lambda: pass_token(q))
+
+    def run_end(layer):
         begin(layer)
         o_relay(layer, 1)
-        lax.fori_loop(0, SECOND_DILATION, angles, 0)
-        pl.when(stays)(turn_tokens)
         todo = events(layer)
-        for q in range(3):
-            handle(layer, todo[q])
-            pl.when(moves)(lambda q=q: pass_token(q))
+        moves_pass(0)
+        moves_pass(1)
+        pl.when(stays)(turn)
+        handle(layer, todo[0])
+        moves_pass(2)
+        handle(layer, todo[1])
+        moves_pass(3)
+        handle(layer, todo[2])
+        pl.when(moves)(turn)
+        if layer == 0:
+            key_value(0)
+        else:
+            query()
+            ask().start()
         o_relay(layer, 2)
-        split = 9 if layer == 2 else 6 if layer != 1 else 7
-        downs = [i for i, event in enumerate(todo) if event[1:3] == ("down", downward[1])]
-        for i in range(3, split):
-            handle(layer, todo[i])
-            if i == 3:
-                pl.when(moves)(lambda: pass_token(3))
-            if layer == 2 and i == max(max(downs), 3):
-                last_down(layer)
-        late = todo[split:]
-        if layer == 1:
-            @pl.when(moves)
-            def _():
-                last_down(layer)
-                for event in late:
-                    handle(layer, event)
-
+        for event in todo[3:6]:
+            handle(layer, event)
         o_relay(layer, 3)
         o_share(0).start()
-        pl.when(moves)(turn_tokens)
-        if layer == last:
-            query()
-            ask().start()
-            key_value(0)
-        else:
-            key_value(0)
-            key_value(1)
-            halos()
-        o_share(0).wait()
-        o_share(1).start()
-        if layer == 1:
-            @pl.when(stays)
-            def _():
-                last_down(layer)
-                for event in late:
-                    handle(layer, event)
-        else:
-            for event in late:
-                handle(layer, event)
-        if layer == last:
+        if layer == 0:
             key_value(1)
             halos()
         else:
+            key_value(0)
+        o_share(0).wait()
+        o_share(1).start()
+        for event in todo[6:]:
+            handle(layer, event)
+        if layer == 0:
             query()
+        else:
+            key_value(1)
+            halos()
+
+    def run_mid(layer):
+        begin(layer)
+        o_relay(layer, 1)
+        todo = events(layer)
+        split = 9 if layer == last - 1 else 7
+        downs = [i for i, event in enumerate(todo) if event[1:3] == ("down", downward[1])]
+        for i in range(split):
+            handle(layer, todo[i])
+            if i < 4:
+                moves_pass(i)
+            if i == 1:
+                pl.when(stays)(turn)
+            if i == 3:
+                o_relay(layer, 2)
+            if layer == last - 1 and i == max(downs):
+                last_down(layer)
+        late = todo[split:]
+
+        def finish():
+            if late:
+                last_down(layer)
+            for event in late:
+                handle(layer, event)
+
+        o_share(0).start()
+        pl.when(moves)(finish)
+        pl.when(moves)(turn)
+        key_value(0)
+        key_value(1)
+        halos()
+        o_share(0).wait()
+        o_share(1).start()
+        pl.when(stays)(finish)
+        query()
+
+    def run(layer):
+        (run_mid if 0 < layer < last else run_end)(layer)
 
     for layer in range(nz):
         pl.when(z == layer)(functools.partial(run, layer))
@@ -725,15 +756,15 @@
     o_share(2).wait()
     for h in range(4):
         pltpu.make_async_copy(heads_in.at[h], heads_in.at[h], head_r.at[h]).wait()
+    merged = jnp.concatenate([heads_in[h] for h in range(4)], axis=1)
+    width = w_out.shape[1]
     for zz in range(nz):
         for yy in range(2):
-            acc = None
-            for h in range(4):
-                one = jnp.dot(heads_in[h], out_rows[h % 2, yy, h // 2, zz], preferred_element_type=jnp.float32)
-                acc = one if acc is None else acc + one
-            width = w_out.shape[1]
+            rows = jnp.concatenate([out_rows[h % 2, yy, h // 2, zz] for h in range(4)], axis=0)
             s = 2 * zz + yy
-            out[:, s * width : (s + 1) * width] = acc.astype(jnp.bfloat16)
+            out[:, s * width : (s + 1) * width] = jnp.dot(
+                merged, rows, preferred_element_type=jnp.float32
+            ).astype(jnp.bfloat16)
 
     for k in range(4):
         pl.when(jnp.logical_not(stays & (tp == k)))(lambda k=k: deal(k).wait_send())

time: 68.1 us -> 63.8 us (0.937)
  the two profiles are of different devices: /device:TPU:9 before, /device:TPU:25 now
where the time goes in v4:
time: 63.8 us; the launch traced here: 63.7 us
  Pallas kernels  61.8 us (97%)
  local copies, waits for them, and re-layouts  1.88 us (3%)
    pallas_call x1, Pallas kernels, one_kernel(): pl.pallas_call(functools.partial(layer_kernel, nz), out_shape=jax.ShapeDt...  61.8 us
    unnamed x1, local copies, waits for them, and re-layouts  1.88 us

profile of v4, /device:TPU:25, one launch (start us, length us, event | category | flops | bytes accessed | tf_op | source)
XLA Modules:
  0.0 63.7 jit_solution(97501999940533956)
XLA Ops:
  0.0 61.8 %shard_map.55 = bf16[128,2048]{1,0:T(8,128)(2,1)} custom-call(bf16[512,2048]{1,0:T(8,128)(2,1)} %tokens.1, bf16[256,384]{1,0:T(8,128)(2,1)} %w_key.1, bf16[256,384]{1,0:T(8,128)(2,1)} %w_value.1, bf16[256,384]{1,0:T(8,128)(2,1)} %w_query.1, bf16[128,256]{1,0:T(8,128)(2,1)} %w_out.1), custom_call_target="tpu_custom_call" | custom-call | tf_op jit(solution)/shard_map/pallas_call | solution.py:820
  61.8 1.9 %copy.7 = bf16[128,2048]{1,0:T(8,128)(2,1)} copy(bf16[128,2048]{1,0:T(8,128)(2,1)} %shard_map.55) | data formatting | bytes 1048576

commit v5 on v4

--- a/solution.py
+++ b/solution.py
@@ -162,7 +162,7 @@
     nz,
     tokens, w_key, w_value, w_query, w_out, out,
     weights, stage, tok_in, tok_turned, cosine, sine, queries, pair0, near_own, near_in, far2,
-    out_rows, mine, heads_in, got01, top01, sum01, asked, part, part_log, got_part, got_log,
+    out_rows, mine, heads_in, got01, top01, sum01, asked, part, part_log, got_part, got_log, begun,
     stage_s, swap_s, tok_k, t_r, ty_s, tx_s, w_r, up_s, down_s, side_s, o_r, o_s, o_r2, far_s, far_r, near_s, near_r, head_s, head_r, part_s, part_r,
 ):
     tok_rows, depth = tokens.shape
@@ -377,10 +377,23 @@
 
         lax.fori_loop(0, depth // 256, piece, 0)
 
-    def project(a, store):
+    def product(both, a, span):
+        return jnp.dot(tok_turned[both, span], weights[a, span, :], preferred_element_type=jnp.float32)
+
+    def start_product(a, span):
         def piece(index, carry):
             both = pl.ds(pl.multiple_of(index * 2 * block, 2 * block), 2 * block)
-            whole = jnp.dot(tok_turned[both, :], weights[a], preferred_element_type=jnp.float32)
+            begun[both, :] = product(both, a, span)
+            return carry
+
+        lax.fori_loop(0, SECOND_DILATION // 2, piece, 0, unroll=2)
+
+    def project(a, store, rest=None):
+        def piece(index, carry):
+            both = pl.ds(pl.multiple_of(index * 2 * block, 2 * block), 2 * block)
+            whole = product(both, a, slice(0, depth) if rest is None else rest)
+            if rest is not None:
+                whole = whole + begun[both, :]
             for k in range(2):
                 rows = pl.ds(pl.multiple_of((2 * index + k) * block, block), block)
                 for g in range(GROUPS):
@@ -412,8 +425,8 @@
     def keep_query(index, rows, g, part):
         queries[g, rows, :] = part.astype(jnp.bfloat16)
 
-    def others(a):
-        for zz in range(nz):
+    def others(a, layers=None):
+        for zz in range(nz) if layers is None else layers:
             s = 2 * zz + 1 - c
             send(chunk(a, s), chunk(a, s), side_s.at[a, zz], w_r.at[a, s], side).wait_recv()
 
@@ -468,40 +481,43 @@
 
     def near_groups():
         def piece(index, carry):
-            begin = index * block
-            rows = pl.ds(pl.multiple_of(begin, block), block)
-            q = queries[0, rows, :]
+            both = pl.ds(pl.multiple_of(index * 2 * block, 2 * block), 2 * block)
+            q = queries[0, both, :]
             tails = pl.ds(tok_rows, tail)
             scores = jnp.concatenate([dots(q, near_in[0, tails, :]), dots(q, pair0[0])], axis=1)
             lane = iota((1, tail + tok_rows), 1)
             time_k = jnp.where(lane < tail, tail_time(lane & (tail - 1)), row_time(lane - tail))
-            time_q = row_time(iota((block, 1), 0) + begin)
-            top0, sum0, weight = soft(scores, time_q, time_k, WIN1, -rank * tok_rows)
-            got0 = jnp.dot(weight[:, :tail], near_in[1, tails, :], preferred_element_type=jnp.float32)
-            got0 += jnp.dot(weight[:, tail:], pair0[1], preferred_element_type=jnp.float32)
-            q = queries[1, rows, :]
-            scores = jnp.concatenate(
-                [dots(q, near_in[0, rows, :]), dots(q, near_own[0, rows, :])], axis=1
-            )
+            time_q = row_time(iota((2 * block, 1), 0) + index * 2 * block)
+            tops, sums, weight = soft(scores, time_q, time_k, WIN1, -rank * tok_rows)
+            gots = jnp.dot(weight[:, :tail], near_in[1, tails, :], preferred_element_type=jnp.float32)
+            gots += jnp.dot(weight[:, tail:], pair0[1], preferred_element_type=jnp.float32)
 
             def step_of(place):
                 return 4 * (place & (sub - 1)) + (place >> sub_log)
 
             lane = iota((1, 2 * block), 1)
             step_k = step_of(lane & (block - 1)) + jnp.where(lane < block, -block, 0)
-            top1, sum1, weight = soft(
-                scores, step_of(iota((block, 1), 0)), step_k, WIN2 // SECOND_DILATION, -rank * block
-            )
-            got1 = jnp.dot(weight[:, :block], near_in[1, rows, :], preferred_element_type=jnp.float32)
-            got1 += jnp.dot(weight[:, block:], near_own[1, rows, :], preferred_element_type=jnp.float32)
-            top = jnp.maximum(top0, top1)
-            f0, f1 = jnp.exp(top0 - top), jnp.exp(top1 - top)
-            got01[rows, :] = f0 * got0 + f1 * got1
-            top01[rows, :] = top
-            sum01[rows, :] = f0 * sum0 + f1 * sum1
+            for k in range(2):
+                rows = pl.ds(pl.multiple_of((2 * index + k) * block, block), block)
+                half = slice(k * block, (k + 1) * block)
+                top0, sum0, got0 = tops[half], sums[half], gots[half]
+                q = queries[1, rows, :]
+                scores = jnp.concatenate(
+                    [dots(q, near_in[0, rows, :]), dots(q, near_own[0, rows, :])], axis=1
+                )
+                top1, sum1, weight = soft(
+                    scores, step_of(iota((block, 1), 0)), step_k, WIN2 // SECOND_DILATION, -rank * block
+                )
+                got1 = jnp.dot(weight[:, :block], near_in[1, rows, :], preferred_element_type=jnp.float32)
+                got1 += jnp.dot(weight[:, block:], near_own[1, rows, :], preferred_element_type=jnp.float32)
+                top = jnp.maximum(top0, top1)
+                f0, f1 = jnp.exp(top0 - top), jnp.exp(top1 - top)
+                got01[rows, :] = f0 * got0 + f1 * got1
+                top01[rows, :] = top
+                sum01[rows, :] = f0 * sum0 + f1 * sum1
             return carry
 
-        lax.fori_loop(0, SECOND_DILATION, piece, 0, unroll=4)
+        lax.fori_loop(0, SECOND_DILATION // 2, piece, 0, unroll=2)
 
     def far_piece(index, source, slots, reach_back, first, until=None):
         begin = index * block
@@ -603,13 +619,13 @@
 
         order()
 
-    def key_value(which):
-        others(which)
-        project(which, keep_pair(which))
-
-    def query():
-        others(2)
-        project(2, keep_query)
+    def key_value(which, layers=None, rest=None):
+        others(which, layers)
+        project(which, keep_pair(which), rest)
+
+    def query(layers=None, rest=None):
+        others(2, layers)
+        project(2, keep_query, rest)
 
     def last_down(layer):
         if 0 < layer < last:
@@ -633,8 +649,8 @@
         moves_pass(2)
         handle(layer, todo[1])
         moves_pass(3)
+        pl.when(moves)(turn)
         handle(layer, todo[2])
-        pl.when(moves)(turn)
         if layer == 0:
             key_value(0)
         else:
@@ -667,6 +683,8 @@
         split = 9 if layer == last - 1 else 7
         downs = [i for i, event in enumerate(todo) if event[1:3] == ("down", downward[1])]
         for i in range(split):
+            if i == 8:
+                pl.when(moves)(turn)
             handle(layer, todo[i])
             if i < 4:
                 moves_pass(i)
@@ -681,12 +699,15 @@
         def finish():
             if late:
                 last_down(layer)
-            for event in late:
+            for event in late[:1]:
+                handle(layer, event)
+            if late:
+                pl.when(moves)(turn)
+            for event in late[1:]:
                 handle(layer, event)
 
         o_share(0).start()
         pl.when(moves)(finish)
-        pl.when(moves)(turn)
         key_value(0)
         key_value(1)
         halos()
@@ -845,6 +866,7 @@
             pltpu.VMEM((SECOND_DILATION, 8, DH), jnp.float32),
             pltpu.VMEM((tok_rows, DH), bf),
             pltpu.VMEM((SECOND_DILATION, 8, DH), jnp.float32),
+            pltpu.VMEM((tok_rows, cols), jnp.float32),
             dma((3,)), dma((3,)), dma, dma((2, 4)), dma((4,)), dma((4,)), dma((3, n_sp)), dma((4, nz)), dma((4, nz)), dma((3, nz)),
             dma((nz,)), dma((3,)), dma((3,)),
             dma((5,)), dma((6,)), dma, dma, dma((4,)), dma((4,)), dma((3,)), dma((3,)),

time: 63.8 us -> 63.5 us (level)
  no operation moved by 1% of the time
where the time goes in v5:
time: 63.5 us; the launch traced here: 63.2 us
  Pallas kernels  61.3 us (97%)
  local copies, waits for them, and re-layouts  1.88 us (3%)
    pallas_call x1, Pallas kernels, one_kernel(): pl.pallas_call(functools.partial(layer_kernel, nz), out_shape=jax.ShapeDt...  61.3 us
    unnamed x1, local copies, waits for them, and re-layouts  1.88 us

profile of v5, /device:TPU:25, one launch (start us, length us, event | category | flops | bytes accessed | tf_op | source)
XLA Modules:
  0.0 63.2 jit_solution(2220506181207531868)
XLA Ops:
  0.0 61.3 %shard_map.55 = bf16[128,2048]{1,0:T(8,128)(2,1)} custom-call(bf16[512,2048]{1,0:T(8,128)(2,1)} %tokens.1, bf16[256,384]{1,0:T(8,128)(2,1)} %w_key.1, bf16[256,384]{1,0:T(8,128)(2,1)} %w_value.1, bf16[256,384]{1,0:T(8,128)(2,1)} %w_query.1, bf16[128,256]{1,0:T(8,128)(2,1)} %w_out.1), custom_call_target="tpu_custom_call" | custom-call | tf_op jit(solution)/shard_map/pallas_call | solution.py:841
  61.3 1.9 %copy.7 = bf16[128,2048]{1,0:T(8,128)(2,1)} copy(bf16[128,2048]{1,0:T(8,128)(2,1)} %shard_map.55) | data formatting | bytes 1048576

commit v6 on v5

--- a/solution.py
+++ b/solution.py
@@ -474,10 +474,10 @@
 
     def soft(scores, time_q, time_k, reach, first):
         gap = time_q - jnp.where(time_k >= first, time_k, far_off)
-        scores = jnp.where((gap >= 0) & (gap <= reach), scores * scale, -jnp.inf)
+        scores = jnp.where((gap >= 0) & (gap <= reach), scores, -jnp.inf)
         top = jnp.max(scores, axis=-1, keepdims=True)
-        weight = jnp.exp(scores - top)
-        return top, jnp.sum(weight, axis=-1, keepdims=True), weight.astype(jnp.bfloat16)
+        weight = jnp.exp2((scores - top) * (scale * math.log2(math.e)))
+        return top * scale, jnp.sum(weight, axis=-1, keepdims=True), weight.astype(jnp.bfloat16)
 
     def near_groups():
         def piece(index, carry):

time: 63.5 us -> 63.5 us (level)
  no operation moved by 1% of the time
where the time goes in v6:
time: 63.5 us; the launch traced here: 63.3 us
  Pallas kernels  61.4 us (97%)
  local copies, waits for them, and re-layouts  1.88 us (3%)
    pallas_call x1, Pallas kernels, one_kernel(): pl.pallas_call(functools.partial(layer_kernel, nz), out_shape=jax.ShapeDt...  61.4 us
    unnamed x1, local copies, waits for them, and re-layouts  1.88 us

profile of v6, /device:TPU:25, one launch (start us, length us, event | category | flops | bytes accessed | tf_op | source)
XLA Modules:
  0.0 63.3 jit_solution(7592548558058184650)
XLA Ops:
  0.0 61.4 %shard_map.55 = bf16[128,2048]{1,0:T(8,128)(2,1)} custom-call(bf16[512,2048]{1,0:T(8,128)(2,1)} %tokens.1, bf16[256,384]{1,0:T(8,128)(2,1)} %w_key.1, bf16[256,384]{1,0:T(8,128)(2,1)} %w_value.1, bf16[256,384]{1,0:T(8,128)(2,1)} %w_query.1, bf16[128,256]{1,0:T(8,128)(2,1)} %w_out.1), custom_call_target="tpu_custom_call" | custom-call | tf_op jit(solution)/shard_map/pallas_call | solution.py:841
  61.4 1.9 %copy.7 = bf16[128,2048]{1,0:T(8,128)(2,1)} copy(bf16[128,2048]{1,0:T(8,128)(2,1)} %shard_map.55) | data formatting | bytes 1048576
